TPU v7x, 256 devices: a whole 4x4x8 slice. The times are simulated.
256 devices in a mesh: ep: 64 (over z, x, core), tp: 4 (over y).
Axes of the slice: x: 4, y: 4, z: 8, core: 2. Of those that a mesh axis runs over, the one named last changes fastest.
Arguments:
- filter_value: bfloat16 [65536, 1024], P(('ep', 'tp')), may hold values from -6 to 6
- filter_gate: bfloat16 [65536, 1024], P(('ep', 'tp')), may hold values from -9 to 9
- filter_taps: float32 [31, 1024], replicated, may hold values from -1 to 1
- filter_bias: float32 [1024], replicated, may hold values from -3 to 3
- norm_gain: float32 [1024], replicated, may hold values from 0.1 to 1.9
- norm_shift: float32 [1024], replicated, may hold values from -3 to 3
- out_weight: bfloat16 [1024, 2048], replicated, may hold values from -0.1875 to 0.1875
- out_bias: float32 [2048], replicated, may hold values from -3 to 3
- expert_input: bfloat16 [16384, 2048], P('ep'), may hold values from -6 to 6
- expert_gain: float32 [2048], replicated, may hold values from 0.1 to 1.9
- route_experts: int32 [16384, 2], P('ep'), may hold values from 0 to 63, all different within a row; in each aligned block of 256 rows (0 to 255, 256 to 511, ...) at most 16 rows name the same one
- route_weights: float32 [16384, 2], P('ep'), may hold values from 0.2 to 1
- gate_weights: bfloat16 [64, 2048, 2048], P('ep', None, 'tp'), may hold values from -0.375 to 0.375
- up_weights: bfloat16 [64, 2048, 2048], P('ep', None, 'tp'), may hold values from -0.375 to 0.375
- down_weights: bfloat16 [64, 2048, 2048], P('ep', 'tp'), may hold values from -0.0234375 to 0.0234375
Outputs:
- mixer_out: bfloat16 [65536, 2048], P(('ep', 'tp'))
- expert_out: bfloat16 [16384, 2048], P('ep', 'tp')
Inputs may be any that keep to these rules, and one draw needn't show every extreme that they name: `route_experts`: each row names 2 different experts. Within the rows of one index of ep (aligned blocks of 256 rows) no expert is named by more than 16 rows, a bound that some block reaches.
All inputs are finite; a program needn't handle non-finite values.
Results may differ from a plain program's by a relative error of at most 0.012.
Values may be sent and summed in bfloat16 or wider, within the bound.
A program may use at most 128 MiB of HBM per device.

v0:
```python
import jax
import jax.numpy as jnp
from jax import lax
from jax.sharding import PartitionSpec as P

epsilon = 1e-06
clamp_limit = 7.0
swish_alpha = 1.702


def passed_along(array, axis, by):
    size = lax.axis_size(axis)
    pairs = [(i, i + by) for i in range(size) if 0 <= i + by < size]
    return lax.ppermute(array, axis, pairs)


def gated_filter(
    filter_value, filter_gate, filter_taps, filter_bias, norm_gain, norm_shift, out_weight, out_bias
):
    gated = (
        filter_value.astype(jnp.float32) * jax.nn.sigmoid(filter_gate.astype(jnp.float32))
    ).astype(jnp.bfloat16)
    length = gated.shape[0]
    reach_back = filter_taps.shape[0] - 1
    rim_rows = passed_along(gated[length - reach_back :], ("ep", "tp"), 1)
    padded = jnp.concatenate([rim_rows, gated], 0)
    filtered = jnp.zeros(gated.shape, jnp.float32)
    for offset in range(reach_back + 1):
        filtered = filtered + filter_taps[offset] * padded[offset : offset + length].astype(
            jnp.float32
        )
    filtered = filtered + filter_bias
    average = jnp.mean(filtered, 1, keepdims=True)
    centred = filtered - average
    variance = jnp.mean(centred * centred, 1, keepdims=True)
    normed_filter = centred * lax.rsqrt(variance + epsilon) * norm_gain + norm_shift
    activated = jax.nn.silu(normed_filter).astype(jnp.bfloat16)
    return (jnp.dot(activated, out_weight, preferred_element_type=jnp.float32) + out_bias).astype(
        jnp.bfloat16
    )


def routed_experts(
    expert_input, expert_gain, route_experts, route_weights, gate_weights, up_weights, down_weights
):
    token_values = expert_input.astype(jnp.float32)
    normed = (
        token_values
        * lax.rsqrt(jnp.mean(token_values * token_values, 1, keepdims=True) + epsilon)
        * expert_gain
    ).astype(jnp.bfloat16)
    row_count, per_token = route_experts.shape
    model_width = normed.shape[1]
    experts = lax.axis_size("ep")
    capacity = 2 * row_count * per_token // experts
    flat_ids = route_experts.reshape(-1)
    onehot = (flat_ids[:, None] == jnp.arange(experts, dtype=jnp.int32)[None, :]).astype(jnp.int32)
    earlier = jnp.cumsum(onehot, 0) - onehot
    target = flat_ids * capacity + jnp.sum(earlier * onehot, 1)
    copies = jnp.repeat(normed, per_token, axis=0)
    outgoing = jnp.zeros((experts * capacity, model_width), jnp.bfloat16).at[target].set(copies)
    outgoing = outgoing.reshape(experts, capacity, model_width)
    quarter = capacity // lax.axis_size("tp")
    start_slot = lax.axis_index("tp") * quarter
    own_slots = lax.dynamic_slice_in_dim(outgoing, start_slot, quarter, 1)
    arrived = lax.all_to_all(own_slots, "ep", split_axis=0, concat_axis=0, tiled=True)
    expert_arrived = lax.all_gather(arrived, "tp", axis=1, tiled=True)
    rows_in = expert_arrived.reshape(-1, model_width)
    gate_pre = jnp.dot(rows_in, gate_weights[0], preferred_element_type=jnp.float32)
    up_pre = jnp.dot(rows_in, up_weights[0], preferred_element_type=jnp.float32)
    gate_held = jnp.minimum(gate_pre, clamp_limit)
    up_held = jnp.clip(up_pre, -clamp_limit, clamp_limit)
    hidden = (gate_held * jax.nn.sigmoid(swish_alpha * gate_held) * (up_held + 1.0)).astype(
        jnp.bfloat16
    )
    result = jnp.dot(hidden, down_weights[0], preferred_element_type=jnp.float32).astype(
        jnp.bfloat16
    )
    partial_value = result.reshape(expert_arrived.shape[0], expert_arrived.shape[1], -1)
    send_partial_value = partial_value
    send_partial_value = lax.optimization_barrier(send_partial_value)
    summed = lax.psum_scatter(
        send_partial_value.astype(jnp.float32).astype(jnp.bfloat16),
        "tp",
        scatter_dimension=2,
        tiled=True,
    )
    returned = lax.all_to_all(summed, "ep", split_axis=0, concat_axis=0, tiled=True)
    flat_back = returned.reshape(experts * capacity, -1)
    picked = flat_back[target].astype(jnp.float32).reshape(row_count, per_token, -1)
    return jnp.sum(picked * route_weights[:, :, None], 1).astype(jnp.bfloat16)


def local(
    filter_value,
    filter_gate,
    filter_taps,
    filter_bias,
    norm_gain,
    norm_shift,
    out_weight,
    out_bias,
    expert_input,
    expert_gain,
    route_experts,
    route_weights,
    gate_weights,
    up_weights,
    down_weights,
):
    mixer_out = gated_filter(
        filter_value,
        filter_gate,
        filter_taps,
        filter_bias,
        norm_gain,
        norm_shift,
        out_weight,
        out_bias,
    )
    expert_out = routed_experts(
        expert_input,
        expert_gain,
        route_experts,
        route_weights,
        gate_weights,
        up_weights,
        down_weights,
    )
    return (mixer_out, expert_out)


def solution(mesh):
    in_specs = (
        P(("ep", "tp"), None),
        P(("ep", "tp"), None),
        P(),
        P(),
        P(),
        P(),
        P(),
        P(),
        P("ep", None),
        P(),
        P("ep", None),
        P("ep", None),
        P("ep", None, "tp"),
        P("ep", None, "tp"),
        P("ep", "tp", None),
    )
    out_specs = (P(("ep", "tp"), None), P("ep", "tp"))
    return jax.shard_map(local, mesh=mesh, in_specs=in_specs, out_specs=out_specs, check_vma=False)
```

profile of v0, /device:TPU:1, one launch (start us, length us, event | category | flops | bytes accessed | tf_op | source)
XLA Modules:
  0.0 242.4 jit_solution(2922952192950757383)
XLA Ops:
  7.2 0.0 copy-start
  7.2 0.0 copy-start.2
  7.2 0.0 copy-start.34
  7.2 0.0 all-gather.2.cloned.1.call-start
  7.2 1.0 copy.29
  8.2 0.1 eq.29
  8.4 0.1 eq.25
  8.5 0.7 broadcast_multiply_fusion
  9.2 1.2 reduce-window.6
  10.4 0.2 slice_reduce_fusion
  10.7 0.1 copy.28
  10.8 0.1 mul.499
  11.0 1.5 fusion.1
  12.5 0.0 copy-done.2
  12.5 0.0 copy-done.34
  12.5 0.3 fusion.3
  12.8 2.6 %broadcast_in_dim.5 = bf16[256,2,2048]{2,1,0:T(2,128)(2,1)} broadcast(bf16[256,2048]{1,0:T(8,128)(2,1)S(1)} %fusion.3), dimensions={0,2} | broadcast | bytes 3145728 | tf_op jit(solution)/shard_map/broadcast_in_dim | solution.py:60
  15.4 4.1 %reshape.114 = bf16[512,2048]{1,0:T(8,128)(2,1)} reshape(bf16[256,2,2048]{2,1,0:T(2,128)(2,1)} %broadcast_in_dim.5) | data formatting | bytes 4194304 | tf_op jit(solution)/shard_map/reshape | solution.py:60
  19.6 0.1 fusion.51
  19.7 0.0 copy-start.35
  19.7 7.2 %scatter_custom_fusion = bf16[1024,2048]{1,0:T(8,128)(2,1)} fusion(s32[512]{0:T(512)S(1)} %bitcast.109, bf16[512,2048]{1,0:T(8,128)(2,1)} %reshape.114, bf16[]{:T(256)} %constant.18.clone.1), kind=kCustom, calls=%fused_computation.45 | custom fusion | bytes 4194816 | tf_op jit(solution)/shard_map/scatter | solution.py:61
  26.9 0.0 copy-done.35
  26.9 2.3 constant_dynamic-slice_fusion
  29.2 40.9 %all_to_all.10 = bf16[64,4,2048]{2,1,0:T(4,128)(2,1)S(1)} all-to-all(bf16[64,4,2048]{2,1,0:T(4,128)(2,1)S(1)} %constant_dynamic-slice_fusion), channel_id=1, replica_groups=mesh['ep'=64,'tp'=4] {'ep'}, dimensions={0} | all-to-all | bytes 2097152 | tf_op jit(solution)/shard_map/all_to_all | solution.py:66
  70.1 1.5 copy.32
  71.7 0.0 all-gather.2.cloned.1.call-update
  71.7 0.2 reduce-scatter.2.cloned.1.call-start
  72.0 47.6 %all-gather.2.cloned.1.call-done = bf16[64,16,2048]{2,0,1:T(8,128)(2,1)} async-done(((bf16[64,4,2048]{2,0,1:T(8,128)(2,1)}), bf16[64,16,2048]{2,0,1:T(8,128)(2,1)}) %all-gather.2.cloned.1.call-update) | async-done | bytes 4194320 | tf_op jit(solution)/shard_map/all_gather | solution.py:67
  119.6 4.6 %copy.33 = bf16[64,16,2048]{2,1,0:T(8,128)(2,1)S(1)} copy(bf16[64,16,2048]{2,0,1:T(8,128)(2,1)} %all-gather.2.cloned.1.call-done) | data formatting | bytes 8388608 | tf_op jit(solution)/shard_map/all_gather | solution.py:67
  124.2 0.0 copy-start.1
  124.2 2.0 copy-done.1
  126.2 0.0 copy-done.37
  126.2 3.7 %fusion.5 = f32[1024,512]{1,0:T(8,128)} fusion(bf16[1024,2048]{1,0:T(8,128)(2,1)S(1)} %bitcast.75, bf16[1,2048,512]{2,1,0:T(8,128)(2,1)S(1)} %copy-done.37), kind=kOutput, calls=%fused_computation.40 | convolution fusion | flops 2147483648 | bytes 8388608 | tf_op jit(solution)/shard_map/dot_general | solution.py:70
  129.9 0.0 copy-done
  129.9 10.3 %convolution_convert_fusion = bf16[1024,2048]{1,0:T(8,128)(2,1)} fusion(bf16[1,512,2048]{2,1,0:T(8,128)(2,1)S(1)} %copy-done, f32[1024,512]{1,0:T(8,128)} %fusion.5, bf16[1024,2048]{1,0:T(8,128)(2,1)} %bitcast.76, bf16[1,2048,512]{2,1,0:T(8,128)(2,1)} %param.27), kind=kOutput, calls=%fused_computation.31 | convolution fusion | flops 4302307328 | bytes 14680064 | tf_op jit(solution)/shard_map/dot_general | solution.py:76
  140.2 0.0 reduce-scatter.2.cloned.1.call-update
  140.2 1.0 copy-done.4
  141.2 0.2 copy-done.5
  141.4 0.3 multiply_convert_fusion.2
  141.7 0.0 copy-start.3
  141.7 0.8 copy-done.3
  142.5 2.5 %collective-permute-start = (bf16[30,1024]{1,0:T(8,128)(2,1)S(1)}, bf16[30,1024]{1,0:T(8,128)(2,1)S(1)}, u32[]{:S(2)}, u32[]{:S(2)}) collective-permute-start(bf16[30,1024]{1,0:T(8,128)(2,1)S(1)} %slice.258), channel_id=1, source_target_pairs={{0,1},{1,2},{2,3},{3,4},{4,5},{5,6},{6,7},{7,8},{8,9},{9,10},{10,1... | collective-permute-start | bytes 184328 | tf_op jit(solution)/shard_map/ppermute | solution.py:14
  145.0 0.0 copy-done.36
  145.0 0.1 copy.34
  145.2 0.0 copy-done.6
  145.2 0.6 fusion.60
  145.8 0.7 fusion.59
  146.5 0.0 copy-start.8
  146.5 0.0 copy-start.9
  146.5 0.0 copy-start.10
  146.5 0.0 copy-start.11
  146.5 0.0 copy-start.12
  146.5 0.0 copy-start.13
  146.7 0.6 pad_clamp_fusion
  147.4 42.9 %reduce-scatter.2.cloned.1.call-done = bf16[64,16,512]{2,1,0:T(8,128)(2,1)} async-done(((bf16[64,16,2048]{2,1,0:T(8,128)(2,1)}), bf16[64,16,512]{2,1,0:T(8,128)(2,1)}) %reduce-scatter.2.cloned.1.call-update) | async-done | bytes 1048592 | tf_op jit(solution)/shard_map/reduce_scatter | solution.py:82
  190.3 10.7 %all-to-all-start.1 = ((bf16[64,16,512]{2,1,0:T(8,128)(2,1)}), bf16[64,16,512]{2,1,0:T(8,128)(2,1)S(1)}, u32[]{:S(2)}, u32[]{:S(2)}) async-start(bf16[64,16,512]{2,1,0:T(8,128)(2,1)} %reduce-scatter.2.cloned.1.call-done), calls=%async_computation.2 | async-start | bytes 2097152 | tf_op jit(solution)/shard_map/all_to_all | solution.py:88
  201.0 0.0 collective-permute-done
  201.3 20.8 %fusion.58 = (f32[256]{0:T(256)S(1)}, f32[256,1024]{1,0:T(8,128)S(1)}) fusion(f32[1024]{0:T(1024)} %param.18, bf16[256,1024]{1,0:T(8,128)(2,1)} %copy-done.3, f32[1024]{0:T(1024)S(1)} %bitcast.87, bf16[30,1024]{1,0:T(8,128)(2,1)S(1)} %collective-permute-done, f32[1024]{0:T(1024)S(1)} %bitcast.88, f32[1024]{0:T(1024)S(1)} %bitcast.90, f32[1024]{0:T(1024)S(1)} %bitcast.91, ...), kind=kLoop, calls=%fused_computation.116 | loop fusion | flops 48234240 | bytes 1766400 | tf_op jit(solution)/shard_map/reduce_sum | solution.py:33
  222.1 0.2 multiply_reduce_fusion.1
  222.4 4.7 %fusion = bf16[256,2048]{1,0:T(8,128)(2,1)} fusion(bf16[1024,2048]{1,0:T(8,128)(2,1)} %param.21, f32[2048]{0:T(1024)S(1)} %copy-done.38, f32[256,1024]{1,0:T(8,128)S(1)} %get-tuple-element.3, f32[1024]{0:T(1024)S(1)} %copy-done.39, f32[1024]{0:T(1024)} %param.19, f32[256]{0:T(256)S(1)} %add_rsqrt_fusion.1, f32[256]{0:T(256)S(1)} %broadcast_multiply_fusion.1), kind=kOutput, calls=%fused_computation.35 | convolution fusion | flops 1077149696 | bytes 6309888 | tf_op jit(solution)/shard_map/dot_general | solution.py:38
  227.1 2.1 all-to-all-done.1
  229.2 2.6 %gather_fusion = bf16[512,512]{1,0:T(8,128)(2,1)} fusion(bf16[1024,512]{1,0:T(8,128)(2,1)S(1)} %bitcast.72, s32[1024]{0:T(1024)S(1)} %pad_clamp_fusion), kind=kCustom, calls=%fused_computation | custom fusion | bytes 1050624 | tf_op jit(solution)/shard_map/gather | solution.py:90
  231.8 1.7 reshape.101
  233.5 2.1 multiply_reduce_fusion
  (65 shorter events, 0.2 us)
Async XLA Ops:
  7.2 122.8 %copy-start = (bf16[1,512,2048]{2,1,0:T(8,128)(2,1)S(1)}, bf16[1,512,2048]{2,1,0:T(8,128)(2,1)}, u32[]{:S(2)}) copy-start(bf16[1,512,2048]{2,1,0:T(8,128)(2,1)} %param.29) | copy-start | bytes 6291460
  7.2 5.3 %copy-start.2 = (bf16[256,2048]{1,0:T(8,128)(2,1)S(1)}, bf16[256,2048]{1,0:T(8,128)(2,1)}, u32[]{:S(2)}) copy-start(bf16[256,2048]{1,0:T(8,128)(2,1)} %param.23) | copy-start | bytes 3145732
  7.2 5.3 %copy-start.34 = (f32[2048]{0:T(1024)S(1)}, f32[2048]{0:T(1024)}, u32[]{:S(2)}) copy-start(f32[2048]{0:T(1024)} %param.24) | copy-start | bytes 24580
  7.2 112.4 %all-gather.2.cloned.1.call-start = ((), (), s32[]{:S(2)}) async-start(), calls=%async_computation.3 | async-start | bytes 5242880 | tf_op jit(solution)/shard_map/all_gather | solution.py:67
  19.7 7.2 %copy-start.35 = (s32[512,1]{0,1:T(1,128)}, s32[512,1]{0,1:T(1,128)S(1)}, u32[]{:S(2)}) copy-start(s32[512,1]{0,1:T(1,128)S(1)} %compare_select_fusion) | copy-start | bytes 6148
  71.7 118.5 %reduce-scatter.2.cloned.1.call-start = ((), (), s32[]{:S(2)}) async-start(), calls=%async_computation.4 | async-start | bytes 5242880 | tf_op jit(solution)/shard_map/reduce_scatter | solution.py:82
  119.6 6.6 %copy-start.37 = (bf16[1,2048,512]{2,1,0:T(8,128)(2,1)S(1)}, bf16[1,2048,512]{2,1,0:T(8,128)(2,1)}, u32[]{:S(2)}) copy-start(bf16[1,2048,512]{2,1,0:T(8,128)(2,1)} %param.28) | copy-start | bytes 6291460
  124.2 2.0 copy-start.1
  140.2 1.0 copy-start.4
  140.2 1.2 copy-start.5
  140.2 4.8 %copy-start.36 = (f32[256,2]{0,1:T(2,128)S(1)}, f32[256,2]{0,1:T(2,128)}, u32[]{:S(2)}) copy-start(f32[256,2]{0,1:T(2,128)} %param.26) | copy-start | bytes 6148
  140.2 4.9 %copy-start.6 = (f32[31,1024]{1,0:T(8,128)S(1)}, f32[31,1024]{1,0:T(8,128)}, u32[]{:S(2)}) copy-start(f32[31,1024]{1,0:T(8,128)} %param.17) | copy-start | bytes 380932
  141.7 0.8 copy-start.3
  142.5 58.5 %collective-permute-start = (bf16[30,1024]{1,0:T(8,128)(2,1)S(1)}, bf16[30,1024]{1,0:T(8,128)(2,1)S(1)}, u32[]{:S(2)}, u32[]{:S(2)}) collective-permute-start(bf16[30,1024]{1,0:T(8,128)(2,1)S(1)} %slice.258), channel_id=1, source_target_pairs={{0,1},{1,2},{2,3},{3,4},{4,5},{5,6},{6,7},{7,8},{8,9},{9,10},{10,1... | collective-permute-start | bytes 184328 | tf_op jit(solution)/shard_map/ppermute | solution.py:14
  146.5 54.5 %copy-start.7 = (f32[1,1024]{1,0:T(1,128)S(1)}, f32[1,1024]{1,0:T(1,128)}, u32[]{:S(2)}) copy-start(f32[1,1024]{1,0:T(1,128)} %get-tuple-element.27) | copy-start | bytes 12292
  146.5 54.5 %copy-start.8 = (f32[1,1024]{1,0:T(1,128)S(1)}, f32[1,1024]{1,0:T(1,128)}, u32[]{:S(2)}) copy-start(f32[1,1024]{1,0:T(1,128)} %get-tuple-element.28) | copy-start | bytes 12292
  146.5 54.5 %copy-start.9 = (f32[1,1024]{1,0:T(1,128)S(1)}, f32[1,1024]{1,0:T(1,128)}, u32[]{:S(2)}) copy-start(f32[1,1024]{1,0:T(1,128)} %get-tuple-element.29) | copy-start | bytes 12292
  146.5 54.5 %copy-start.10 = (f32[1,1024]{1,0:T(1,128)S(1)}, f32[1,1024]{1,0:T(1,128)}, u32[]{:S(2)}) copy-start(f32[1,1024]{1,0:T(1,128)} %get-tuple-element.30) | copy-start | bytes 12292
  146.5 54.5 %copy-start.11 = (f32[1,1024]{1,0:T(1,128)S(1)}, f32[1,1024]{1,0:T(1,128)}, u32[]{:S(2)}) copy-start(f32[1,1024]{1,0:T(1,128)} %get-tuple-element.31) | copy-start | bytes 12292
  146.5 54.5 %copy-start.12 = (f32[1,1024]{1,0:T(1,128)S(1)}, f32[1,1024]{1,0:T(1,128)}, u32[]{:S(2)}) copy-start(f32[1,1024]{1,0:T(1,128)} %get-tuple-element.32) | copy-start | bytes 12292
  146.5 54.5 %copy-start.13 = (f32[1,1024]{1,0:T(1,128)S(1)}, f32[1,1024]{1,0:T(1,128)}, u32[]{:S(2)}) copy-start(f32[1,1024]{1,0:T(1,128)} %get-tuple-element.33) | copy-start | bytes 12292
  146.5 54.5 %copy-start.14 = (f32[1,1024]{1,0:T(1,128)S(1)}, f32[1,1024]{1,0:T(1,128)}, u32[]{:S(2)}) copy-start(f32[1,1024]{1,0:T(1,128)} %get-tuple-element.34) | copy-start | bytes 12292
  146.5 54.5 %copy-start.15 = (f32[1,1024]{1,0:T(1,128)S(1)}, f32[1,1024]{1,0:T(1,128)}, u32[]{:S(2)}) copy-start(f32[1,1024]{1,0:T(1,128)} %get-tuple-element.4) | copy-start | bytes 12292
  146.6 54.5 %copy-start.16 = (f32[1,1024]{1,0:T(1,128)S(1)}, f32[1,1024]{1,0:T(1,128)}, u32[]{:S(2)}) copy-start(f32[1,1024]{1,0:T(1,128)} %get-tuple-element.5) | copy-start | bytes 12292
  146.6 54.5 %copy-start.17 = (f32[1,1024]{1,0:T(1,128)S(1)}, f32[1,1024]{1,0:T(1,128)}, u32[]{:S(2)}) copy-start(f32[1,1024]{1,0:T(1,128)} %get-tuple-element.6) | copy-start | bytes 12292
  146.6 54.5 %copy-start.18 = (f32[1,1024]{1,0:T(1,128)S(1)}, f32[1,1024]{1,0:T(1,128)}, u32[]{:S(2)}) copy-start(f32[1,1024]{1,0:T(1,128)} %get-tuple-element.7) | copy-start | bytes 12292
  146.6 54.5 %copy-start.19 = (f32[1,1024]{1,0:T(1,128)S(1)}, f32[1,1024]{1,0:T(1,128)}, u32[]{:S(2)}) copy-start(f32[1,1024]{1,0:T(1,128)} %get-tuple-element.8) | copy-start | bytes 12292
  146.6 54.5 %copy-start.20 = (f32[1,1024]{1,0:T(1,128)S(1)}, f32[1,1024]{1,0:T(1,128)}, u32[]{:S(2)}) copy-start(f32[1,1024]{1,0:T(1,128)} %get-tuple-element.9) | copy-start | bytes 12292
  146.6 54.5 %copy-start.21 = (f32[1,1024]{1,0:T(1,128)S(1)}, f32[1,1024]{1,0:T(1,128)}, u32[]{:S(2)}) copy-start(f32[1,1024]{1,0:T(1,128)} %get-tuple-element.10) | copy-start | bytes 12292
  146.6 54.5 %copy-start.22 = (f32[1,1024]{1,0:T(1,128)S(1)}, f32[1,1024]{1,0:T(1,128)}, u32[]{:S(2)}) copy-start(f32[1,1024]{1,0:T(1,128)} %get-tuple-element.11) | copy-start | bytes 12292
  146.6 54.5 %copy-start.23 = (f32[1,1024]{1,0:T(1,128)S(1)}, f32[1,1024]{1,0:T(1,128)}, u32[]{:S(2)}) copy-start(f32[1,1024]{1,0:T(1,128)} %get-tuple-element.12) | copy-start | bytes 12292
  146.6 54.5 %copy-start.24 = (f32[1,1024]{1,0:T(1,128)S(1)}, f32[1,1024]{1,0:T(1,128)}, u32[]{:S(2)}) copy-start(f32[1,1024]{1,0:T(1,128)} %get-tuple-element.13) | copy-start | bytes 12292
  146.6 54.5 %copy-start.25 = (f32[1,1024]{1,0:T(1,128)S(1)}, f32[1,1024]{1,0:T(1,128)}, u32[]{:S(2)}) copy-start(f32[1,1024]{1,0:T(1,128)} %get-tuple-element.14) | copy-start | bytes 12292
  146.7 54.5 %copy-start.26 = (f32[1,1024]{1,0:T(1,128)S(1)}, f32[1,1024]{1,0:T(1,128)}, u32[]{:S(2)}) copy-start(f32[1,1024]{1,0:T(1,128)} %get-tuple-element.15) | copy-start | bytes 12292
  146.7 54.5 %copy-start.27 = (f32[1,1024]{1,0:T(1,128)S(1)}, f32[1,1024]{1,0:T(1,128)}, u32[]{:S(2)}) copy-start(f32[1,1024]{1,0:T(1,128)} %get-tuple-element.16) | copy-start | bytes 12292
  146.7 54.5 %copy-start.28 = (f32[1,1024]{1,0:T(1,128)S(1)}, f32[1,1024]{1,0:T(1,128)}, u32[]{:S(2)}) copy-start(f32[1,1024]{1,0:T(1,128)} %get-tuple-element.17) | copy-start | bytes 12292
  146.7 54.5 %copy-start.29 = (f32[1,1024]{1,0:T(1,128)S(1)}, f32[1,1024]{1,0:T(1,128)}, u32[]{:S(2)}) copy-start(f32[1,1024]{1,0:T(1,128)} %get-tuple-element.18) | copy-start | bytes 12292
  146.7 54.5 %copy-start.30 = (f32[1,1024]{1,0:T(1,128)S(1)}, f32[1,1024]{1,0:T(1,128)}, u32[]{:S(2)}) copy-start(f32[1,1024]{1,0:T(1,128)} %get-tuple-element.19) | copy-start | bytes 12292
  146.7 54.5 %copy-start.31 = (f32[1,1024]{1,0:T(1,128)S(1)}, f32[1,1024]{1,0:T(1,128)}, u32[]{:S(2)}) copy-start(f32[1,1024]{1,0:T(1,128)} %get-tuple-element.20) | copy-start | bytes 12292
  146.7 54.5 %copy-start.32 = (f32[1,1024]{1,0:T(1,128)S(1)}, f32[1,1024]{1,0:T(1,128)}, u32[]{:S(2)}) copy-start(f32[1,1024]{1,0:T(1,128)} %get-tuple-element.21) | copy-start | bytes 12292
  146.7 54.5 %copy-start.33 = (f32[1,1024]{1,0:T(1,128)S(1)}, f32[1,1024]{1,0:T(1,128)}, u32[]{:S(2)}) copy-start(f32[1,1024]{1,0:T(1,128)} %get-tuple-element.22) | copy-start | bytes 12292
  147.4 75.0 %copy-start.38 = (f32[2048]{0:T(1024)S(1)}, f32[2048]{0:T(1024)}, u32[]{:S(2)}) copy-start(f32[2048]{0:T(1024)} %param.22) | copy-start | bytes 24580
  147.4 75.0 %copy-start.39 = (f32[1024]{0:T(1024)S(1)}, f32[1024]{0:T(1024)}, u32[]{:S(2)}) copy-start(f32[1024]{0:T(1024)} %param.20) | copy-start | bytes 12292
  190.3 38.9 %all-to-all-start.1 = ((bf16[64,16,512]{2,1,0:T(8,128)(2,1)}), bf16[64,16,512]{2,1,0:T(8,128)(2,1)S(1)}, u32[]{:S(2)}, u32[]{:S(2)}) async-start(bf16[64,16,512]{2,1,0:T(8,128)(2,1)} %reduce-scatter.2.cloned.1.call-done), calls=%async_computation.2 | async-start | bytes 2097152 | tf_op jit(solution)/shard_map/all_to_all | solution.py:88
Sparse Core Ops, SparseCore 0:
  71.8 47.6 all-gather.1
  140.4 49.8 reduce-scatter.1
where the time goes:
time: 243 us; the launch traced here: 242 us
  waiting for transfers between devices  92.6 us (38%)
  blocking collectives  40.9 us (17%)
  local copies, waits for them, and re-layouts  34 us (14%)
  other arithmetic  27.9 us (11%)
  matrix products  18.7 us (8%)
  between operations  14.7 us (6%)
  starting transfers between devices  13.5 us (6%)
    all_gather x1, waiting for transfers between devices, routed_experts(): expert_arrived = lax.all_gather(arrived, 'tp', axis=1, tiled=True)  47.6 us
    reduce_scatter x1, waiting for transfers between devices, routed_experts(): lax.psum_scatter(send_partial_value.astype(jnp.float32).astype(jnp.bfloat...  42.9 us
    all_to_all x1, blocking collectives, routed_experts(): lax.all_to_all(own_slots, 'ep', split_axis=0, concat_axis=0, tiled=True)  40.9 us
    reduce_sum x1, other arithmetic, gated_filter(): average = jnp.mean(filtered, 1, keepdims=True)  20.8 us
    all_to_all x1, starting transfers between devices, routed_experts(): lax.all_to_all(summed, 'ep', split_axis=0, concat_axis=0, tiled=True)  10.7 us
    dot_general x1, matrix products, routed_experts(): jnp.dot(hidden, down_weights[0], preferred_element_type=jnp.float32)  10.3 us
    scatter x1, local copies, waits for them, and re-layouts, routed_experts(): jnp.zeros((experts * capacity, model_width), jnp.bfloat16).at[target]  7.22 us
    unnamed x82, local copies, waits for them, and re-layouts  5.2 us
  transfers between devices with their start and end apart: 4, of which 3 were waited for; matrix products, arithmetic and copies ran while one was open for 12% of the time, Pallas kernels for 0%

commit v1 on v0

v1 whole, which is shorter than its diff:
```python
import functools

import jax
import jax.numpy as jnp
from jax import lax
from jax.experimental import pallas as pl
from jax.experimental.pallas import tpu as pltpu
from jax.sharding import PartitionSpec as P

MESH = pl.DeviceIdType.MESH
BF16, F32, I32 = jnp.bfloat16, jnp.float32, jnp.int32

EPS = 1e-06
LIMIT = 7.0
ALPHA = 1.702

NZ = 8
PLANE = 8
NEP = 64
NTP = 4
SLOTS = 16
ROWS = PLANE * SLOTS
TOKENS = 256
WIDTH = 512
HALF = ROWS // 2
ORDER = (0, 1, -2, 2, -3, 3, 4, -1)
TAPS = 31
CHANNELS = 1024
TILE = 64


def copy_to(src, dst, send, recv, device):
    return pltpu.make_async_remote_copy(
        src_ref=src, dst_ref=dst, send_sem=send, recv_sem=recv, device_id=device, device_id_type=MESH
    )


def travel(group):
    value = jnp.int32(ORDER[0])
    for index, by in enumerate(ORDER):
        value = jnp.where(group == index, jnp.int32(by), value)
    return value


def kernel(
    value_ref, gate_ref, taps_ref, fbias_ref, ngain_ref, nshift_ref, ow_hbm, obias_ref,
    xin_ref, egain_ref, routes_ref, rweights_ref, wg_hbm, wu_hbm, wd_hbm,
    mixer_ref, out_ref,
    rm, tk, pick, nb, outgoing, rows_in, wg, wu, wd, ow, parts, first_in, second_out, second_in,
    summed, ret, halo_out, halo_in, gbuf, filt, act,
    load_sem, disp_send, disp_recv, ag_send, ag_recv, fwd_send, fwd_recv,
    rs1_send, rs1_recv, rs2_send, rs2_recv, ret_send, ret_recv, halo_send, halo_recv,
):
    me = lax.axis_index("ep")
    y = lax.axis_index("tp")
    z, own = me // PLANE, me % PLANE
    right, left = (y + 1) % NTP, (y + NTP - 1) % NTP
    line = me * NTP + y
    after = (line + 1) % (NEP * NTP)
    to_right, to_left = {"ep": me, "tp": right}, {"ep": me, "tp": left}
    to_after = {"ep": after // NTP, "tp": after % NTP}

    loads = []
    for k, shift in enumerate((0, 3, 1, 2)):
        at = pl.ds(pl.multiple_of((y + shift) % NTP * WIDTH, WIDTH), WIDTH)
        loads.append(pltpu.make_async_copy(wg_hbm.at[0, at, :], wg.at[k], load_sem.at[k]))
        loads.append(pltpu.make_async_copy(wu_hbm.at[0, at, :], wu.at[k], load_sem.at[4 + k]))
    for k, shift in enumerate((0, 1, 3, 2)):
        at = pl.ds(pl.multiple_of((y + shift) % NTP * WIDTH, WIDTH), WIDTH)
        loads.append(pltpu.make_async_copy(wd_hbm.at[0, :, at], wd.at[k], load_sem.at[8 + k]))
    loads.append(pltpu.make_async_copy(ow_hbm, ow, load_sem.at[12]))
    for load in loads:
        load.start()

    routes = routes_ref[...]
    expert = lax.broadcasted_iota(I32, (NEP, TOKENS), 0)
    named0 = routes[0:1, :] == expert
    named1 = routes[1:2, :] == expert
    named = jnp.logical_or(named0, named1)
    earlier = (
        lax.broadcasted_iota(I32, (TOKENS, TOKENS), 0) < lax.broadcasted_iota(I32, (TOKENS, TOKENS), 1)
    ).astype(F32).astype(BF16)
    rank = jnp.dot(named.astype(F32).astype(BF16), earlier, preferred_element_type=F32)
    rm[...] = jnp.where(named, rank, -1.0).astype(BF16)
    for k, hit in enumerate((named0, named1)):
        weight = jnp.broadcast_to(rweights_ref[k : k + 1, :], (NEP, TOKENS))
        tk[k] = jnp.concatenate([jnp.where(hit, rank, -1.0), weight], 0).T

    columns = pl.ds(pl.multiple_of(y * WIDTH, WIDTH), WIDTH)

    def normed(i, carry):
        at = pl.ds(pl.multiple_of(i * 16, 16), 16)
        tokens = xin_ref[at, :].astype(F32)
        scale = lax.rsqrt(jnp.mean(tokens * tokens, 1, keepdims=True) + EPS)
        nb[at, :] = (xin_ref[at, columns].astype(F32) * scale * egain_ref[0:1, columns]).astype(BF16)
        return carry

    lax.fori_loop(0, TOKENS // 16, normed, 0)

    row = lax.broadcasted_iota(I32, (ROWS, NEP), 0)
    col = lax.broadcasted_iota(I32, (ROWS, NEP), 1)
    slot_row = (lax.broadcasted_iota(I32, (ROWS, TOKENS), 0) % SLOTS).astype(F32)

    def place(group):
        target = (z + travel(group) + NZ) % NZ
        spread = (row // SLOTS + target * PLANE == col).astype(F32).astype(BF16)
        ranks = jnp.dot(spread, rm[...], preferred_element_type=F32)
        chosen = (ranks == slot_row).astype(F32).astype(BF16)
        outgoing[group] = jnp.dot(chosen, nb[...], preferred_element_type=F32).astype(BF16)

    def dispatch(group):
        target = (z + travel(group) + NZ) % NZ

        def one(q, carry):
            index = (own + q) % PLANE
            there = target * PLANE + index
            at = pl.ds(pl.multiple_of(index * SLOTS, SLOTS), SLOTS)
            mine = pl.ds(pl.multiple_of(own * SLOTS, SLOTS), SLOTS)

            @pl.when(there != me)
            def _():
                copy_to(
                    outgoing.at[group, at, :], rows_in.at[0, group, mine, :], disp_send, disp_recv.at[group],
                    {"ep": there, "tp": y},
                ).start()

            @pl.when(there == me)
            def _():
                rows_in[0, group, mine, :] = outgoing[group, mine, :]

            return carry

        lax.fori_loop(0, PLANE, one, 0)

    def place_and_send(group, carry):
        @pl.when(group < NZ)
        def _():
            place(group)

        @pl.when(group > 0)
        def _():
            dispatch(group - 1)

        return carry

    lax.fori_loop(0, NZ + 1, place_and_send, 0)

    def gated(i, carry):
        at = pl.ds(pl.multiple_of(i * 16, 16), 16)
        product = (value_ref[at, :].astype(F32) * jax.nn.sigmoid(gate_ref[at, :].astype(F32))).astype(BF16)
        gbuf[pl.ds(pl.multiple_of(i * 16 + 32, 16), 16), :] = product.astype(F32)

        @pl.when(i >= TOKENS // 16 - 2)
        def _():
            halo_out[pl.ds(pl.multiple_of(i * 16 - (TOKENS - 32), 16), 16), :] = product

        return carry

    lax.fori_loop(0, TOKENS // 16, gated, 0)
    halo = copy_to(halo_out, halo_in, halo_send, halo_recv, to_after)
    halo.start()

    def conv(tile):
        def lanes(block, carry):
            at = pl.ds(pl.multiple_of(block * 128, 128), 128)
            window = gbuf[pl.ds(pl.multiple_of(tile * TILE, TILE), TILE + 32), at]
            total = jnp.broadcast_to(fbias_ref[0:1, at], (TILE, 128))
            for r in range(8):
                moved = window if r == 0 else pltpu.roll(window, TILE + 32 - r, 0)
                for q in range(5):
                    j = 8 * q + r - 2
                    if 0 <= j < TAPS:
                        total = total + taps_ref[j : j + 1, at] * moved[8 * q : 8 * q + TILE]
            filt[:, at] = total
            return carry

        lax.fori_loop(0, CHANNELS // 128, lanes, 0)

        def norm(i, carry):
            at = pl.ds(pl.multiple_of(i * 16, 16), 16)
            rows = filt[at, :]
            centred = rows - jnp.mean(rows, 1, keepdims=True)
            variance = jnp.mean(centred * centred, 1, keepdims=True)
            out = centred * lax.rsqrt(variance + EPS) * ngain_ref[0:1, :] + nshift_ref[0:1, :]
            act[pl.ds(pl.multiple_of(tile * TILE + i * 16, 16), 16), :] = (out * jax.nn.sigmoid(out)).astype(BF16)
            return carry

        lax.fori_loop(0, TILE // 16, norm, 0)

    def project(chunk):
        at = pl.ds(pl.multiple_of(chunk * 512, 512), 512)
        out = jnp.dot(act[...], ow[:, at], preferred_element_type=F32) + obias_ref[0:1, at]
        mixer_ref[:, at] = out.astype(BF16)

    def gather_own(g):
        @pl.when(g == 0)
        def _():
            some = rows_in.at[0, 0, pl.ds(0, ROWS - SLOTS), :]
            copy_to(some, some, disp_send, disp_recv.at[0], to_right).wait_recv()

        @pl.when(g > 0)
        def _():
            every = rows_in.at[0, g]
            copy_to(every, every, disp_send, disp_recv.at[g], to_right).wait_recv()

        copy_to(rows_in.at[0, g], rows_in.at[1, g], ag_send, ag_recv.at[0, g], to_right).start()
        copy_to(rows_in.at[0, g], rows_in.at[2, g], ag_send, ag_recv.at[1, g], to_left).start()

    top, low = pl.ds(0, HALF), pl.ds(HALF, HALF)

    def gather_on(g):
        copy_to(rows_in.at[0, g], rows_in.at[1, g], ag_send, ag_recv.at[0, g], to_right).wait_recv()
        copy_to(rows_in.at[1, g, top, :], rows_in.at[3, g, top, :], fwd_send, fwd_recv.at[g], to_right).start()
        copy_to(rows_in.at[0, g], rows_in.at[2, g], ag_send, ag_recv.at[1, g], to_left).wait_recv()
        copy_to(rows_in.at[2, g, low, :], rows_in.at[3, g, low, :], fwd_send, fwd_recv.at[g], to_left).start()

    def experts(g):
        whole = rows_in.at[3, g]
        copy_to(whole, whole, fwd_send, fwd_recv.at[g], to_right).wait_recv()
        gate_pre = jnp.zeros((ROWS, WIDTH), F32)
        up_pre = jnp.zeros((ROWS, WIDTH), F32)
        for k in range(NTP):
            block = rows_in[k, g]
            gate_pre = gate_pre + jnp.dot(block, wg[k], preferred_element_type=F32)
            up_pre = up_pre + jnp.dot(block, wu[k], preferred_element_type=F32)
        gate_held = jnp.minimum(gate_pre, LIMIT)
        up_held = jnp.clip(up_pre, -LIMIT, LIMIT)
        hidden = (gate_held * jax.nn.sigmoid(ALPHA * gate_held) * (up_held + 1.0)).astype(BF16)
        for k in (3, 1, 2, 0):
            parts[k, g] = jnp.dot(hidden, wd[k], preferred_element_type=F32).astype(BF16)
        copy_to(parts.at[3, g, top, :], first_in.at[0, g], rs1_send, rs1_recv.at[0, g], to_right).start()
        copy_to(parts.at[3, g, low, :], first_in.at[1, g], rs1_send, rs1_recv.at[1, g], to_left).start()

    def reduce_on(g):
        copy_to(parts.at[3, g, top, :], first_in.at[0, g], rs1_send, rs1_recv.at[0, g], to_right).wait_recv()
        second_out[0, g, top, :] = (
            parts[1, g, top, :].astype(F32) + first_in[0, g].astype(F32)
        ).astype(BF16)
        second_out[0, g, low, :] = parts[1, g, low, :]
        copy_to(second_out.at[0, g], second_in.at[0, g], rs2_send, rs2_recv.at[0, g], to_right).start()
        copy_to(parts.at[3, g, low, :], first_in.at[1, g], rs1_send, rs1_recv.at[1, g], to_left).wait_recv()
        second_out[1, g, top, :] = parts[2, g, top, :]
        second_out[1, g, low, :] = (
            parts[2, g, low, :].astype(F32) + first_in[1, g].astype(F32)
        ).astype(BF16)
        copy_to(second_out.at[1, g], second_in.at[1, g], rs2_send, rs2_recv.at[1, g], to_left).start()

    def send_back(g):
        copy_to(second_out.at[0, g], second_in.at[0, g], rs2_send, rs2_recv.at[0, g], to_right).wait_recv()
        copy_to(second_out.at[1, g], second_in.at[1, g], rs2_send, rs2_recv.at[1, g], to_left).wait_recv()
        total = parts[0, g].astype(F32) + second_in[0, g].astype(F32) + second_in[1, g].astype(F32)
        summed[g] = total.astype(BF16)
        source = (z - travel(g) + NZ) % NZ
        mine = pl.ds(pl.multiple_of(me * SLOTS, SLOTS), SLOTS)

        def one(q, carry):
            index = (own + q) % PLANE
            there = source * PLANE + index
            at = pl.ds(pl.multiple_of(index * SLOTS, SLOTS), SLOTS)

            @pl.when(there != me)
            def _():
                copy_to(
                    summed.at[g, at, :], ret.at[mine, :], ret_send, ret_recv, {"ep": there, "tp": y}
                ).start()

            @pl.when(there == me)
            def _():
                ret[mine, :] = summed[g, at, :]

            return carry

        lax.fori_loop(0, PLANE, one, 0)

    def picks():
        lane = lax.broadcasted_iota(I32, (NEP, NEP * SLOTS), 1)
        spread = (lane // SLOTS == lax.broadcasted_iota(I32, (NEP, NEP * SLOTS), 0)).astype(F32).astype(BF16)
        slot = (lax.broadcasted_iota(I32, (TOKENS, NEP * SLOTS), 1) % SLOTS).astype(F32)
        for k in range(2):
            ranks = jnp.dot(tk[k][:, 0:NEP].astype(BF16), spread, preferred_element_type=F32)
            pick[k] = (ranks == slot).astype(F32).astype(BF16)

    def step(t, carry):
        @pl.when(t < NZ)
        def _():
            gather_own(t)

        @pl.when(jnp.logical_and(t >= 1, t < NZ + 1))
        def _():
            gather_on(t - 1)

        @pl.when(t >= 4)
        def _():
            send_back(t - 4)

        @pl.when(jnp.logical_and(t >= 3, t < NZ + 3))
        def _():
            reduce_on(t - 3)

        @pl.when(t == 2)
        def _():
            for load in loads[:12]:
                load.wait()

        @pl.when(jnp.logical_and(t >= 2, t < NZ + 2))
        def _():
            experts(t - 2)

        @pl.when(t == 0)
        def _():
            halo.wait()
            gbuf[0:32, :] = jnp.where(line == 0, 0.0, halo_in[...].astype(F32))

        @pl.when(t < 4)
        def _():
            conv(t)

        @pl.when(t == 4)
        def _():
            loads[12].wait()

        @pl.when(jnp.logical_and(t >= 4, t < 8))
        def _():
            project(t - 4)

        @pl.when(t == 8)
        def _():
            picks()

        return carry

    lax.fori_loop(0, NZ + 4, step, 0)

    but_one = ret.at[pl.ds(0, (NEP - 1) * SLOTS), :]
    copy_to(but_one, but_one, ret_send, ret_recv, to_right).wait_recv()
    expert_out = jnp.zeros((TOKENS, WIDTH), F32)
    for k in range(2):
        picked = jnp.dot(pick[k], ret[...], preferred_element_type=F32)
        expert_out = expert_out + picked * tk[k][:, NEP : NEP + 1]
    out_ref[...] = expert_out.astype(BF16)

    copy_to(but_one, but_one, disp_send, ret_recv, to_right).wait_send()
    copy_to(but_one, but_one, ret_send, ret_recv, to_right).wait_send()
    copy_to(second_in, second_in, ag_send, ret_recv, to_right).wait_send()
    copy_to(second_in, second_in, rs2_send, ret_recv, to_right).wait_send()
    copy_to(first_in, first_in, fwd_send, ret_recv, to_right).wait_send()
    copy_to(first_in, first_in, rs1_send, ret_recv, to_right).wait_send()


def local(
    filter_value, filter_gate, filter_taps, filter_bias, norm_gain, norm_shift, out_weight, out_bias,
    expert_input, expert_gain, route_experts, route_weights, gate_weights, up_weights, down_weights,
):
    vmem = pl.BlockSpec(memory_space=pltpu.VMEM)
    hbm = pl.BlockSpec(memory_space=pl.ANY)
    dma = pltpu.SemaphoreType.DMA
    return pl.pallas_call(
        kernel,
        out_shape=(
            jax.ShapeDtypeStruct((TOKENS, 2048), BF16),
            jax.ShapeDtypeStruct((TOKENS, WIDTH), BF16),
        ),
        in_specs=[vmem] * 6 + [hbm] + [vmem] * 5 + [hbm] * 3,
        out_specs=(vmem, vmem),
        scratch_shapes=[
            pltpu.VMEM((NEP, TOKENS), BF16),
            pltpu.VMEM((2, TOKENS, 2 * NEP), F32),
            pltpu.VMEM((2, TOKENS, NEP * SLOTS), BF16),
            pltpu.VMEM((TOKENS, WIDTH), BF16),
            pltpu.VMEM((NZ, ROWS, WIDTH), BF16),
            pltpu.VMEM((NTP, NZ, ROWS, WIDTH), BF16),
            pltpu.VMEM((NTP, WIDTH, WIDTH), BF16),
            pltpu.VMEM((NTP, WIDTH, WIDTH), BF16),
            pltpu.VMEM((NTP, WIDTH, WIDTH), BF16),
            pltpu.VMEM((CHANNELS, 2048), BF16),
            pltpu.VMEM((NTP, NZ, ROWS, WIDTH), BF16),
            pltpu.VMEM((2, NZ, HALF, WIDTH), BF16),
            pltpu.VMEM((2, NZ, ROWS, WIDTH), BF16),
            pltpu.VMEM((2, NZ, ROWS, WIDTH), BF16),
            pltpu.VMEM((NZ, ROWS, WIDTH), BF16),
            pltpu.VMEM((NEP * SLOTS, WIDTH), BF16),
            pltpu.VMEM((32, CHANNELS), BF16),
            pltpu.VMEM((32, CHANNELS), BF16),
            pltpu.VMEM((TOKENS + 32, CHANNELS), F32),
            pltpu.VMEM((TILE, CHANNELS), F32),
            pltpu.VMEM((TOKENS, CHANNELS), BF16),
            dma((13,)),
            dma, dma((NZ,)), dma, dma((2, NZ)), dma, dma((NZ,)),
            dma, dma((2, NZ)), dma, dma((2, NZ)), dma, dma, dma, dma,
        ],
        compiler_params=pltpu.CompilerParams(has_side_effects=True, vmem_limit_bytes=56 * 1024 * 1024),
        name="filter_and_experts",
    )(
        filter_value, filter_gate, filter_taps, filter_bias[None], norm_gain[None], norm_shift[None],
        out_weight, out_bias[None], expert_input, expert_gain[None], route_experts.T, route_weights.T,
        gate_weights, up_weights, down_weights,
    )


def solution(mesh):
    in_specs = (
        P(("ep", "tp"), None),
        P(("ep", "tp"), None),
        P(),
        P(),
        P(),
        P(),
        P(),
        P(),
        P("ep", None),
        P(),
        P("ep", None),
        P("ep", None),
        P("ep", None, "tp"),
        P("ep", None, "tp"),
        P("ep", "tp", None),
    )
    out_specs = (P(("ep", "tp"), None), P("ep", "tp"))
    return jax.shard_map(local, mesh=mesh, in_specs=in_specs, out_specs=out_specs, check_vma=False)
```

time: 243 us -> 124 us (0.51)
  Pallas kernels: 0 us -> 120 us
  waiting for transfers between devices: 92.6 us -> 0 us
  blocking collectives: 40.9 us -> 0 us
  local copies, waits for them, and re-layouts: 34 us -> 3.05 us
  other arithmetic: 27.9 us -> 0 us
  matrix products: 18.7 us -> 0 us
  between operations: 14.7 us -> 0.65 us
  starting transfers between devices: 13.5 us -> 0 us
    pallas_call x0 -> x1, Pallas kernels: none -> 120 us  [local(): pl.pallas_call(kernel, out_shape=(jax.ShapeDtypeStruct((TOKENS, 2048), BF...]
    all_gather x1 -> x0, waiting for transfers between devices: 47.6 us -> none  [routed_experts(): expert_arrived = lax.all_gather(arrived, 'tp', axis=1, tiled=True)]
    reduce_scatter x1 -> x0, waiting for transfers between devices: 42.9 us -> none  [routed_experts(): lax.psum_scatter(send_partial_value.astype(jnp.float32).astype(jnp.bfloat...]
    all_to_all x1 -> x0, blocking collectives: 40.9 us -> none  [routed_experts(): lax.all_to_all(own_slots, 'ep', split_axis=0, concat_axis=0, tiled=True)]
    reduce_sum x5 -> x0, other arithmetic: 24.7 us -> none  [the longest x1 20.8 us: gated_filter(): average = jnp.mean(filtered, 1, keepdims=True)]
    dot_general x3 -> x0, matrix products: 18.7 us -> none  [the longest x1 10.3 us: routed_experts(): jnp.dot(hidden, down_weights[0], preferred_element_type=jnp.float32)]
    all_to_all x1 -> x0, starting transfers between devices: 10.7 us -> none  [routed_experts(): lax.all_to_all(summed, 'ep', split_axis=0, concat_axis=0, tiled=True)]
    scatter x1 -> x0, local copies, waits for them, and re-layouts: 7.22 us -> none  [routed_experts(): jnp.zeros((experts * capacity, model_width), jnp.bfloat16).at[target]]
  transfers between devices with their start and end apart: 4 -> 0, of which waited for: 3 -> 0; matrix products, arithmetic and copies ran while one was open for 12% -> 0% of each run, Pallas kernels for 0% -> 0%
where the time goes in v1:
time: 124 us
  Pallas kernels  120 us (97%)
  local copies, waits for them, and re-layouts  3.05 us (2%)
    pallas_call x1, Pallas kernels, local(): pl.pallas_call(kernel, out_shape=(jax.ShapeDtypeStruct((TOKENS, 2048), BF...  120 us
    unnamed x4, local copies, waits for them, and re-layouts  3.05 us

profile of v1, /device:TPU:1, one launch (start us, length us, event | category | flops | bytes accessed | tf_op | source)
XLA Modules:
  0.0 124.0 jit_solution(1991042093986704248)
XLA Ops:
  0.6 120.3 %filter_and_experts.1 = (bf16[256,2048]{1,0:T(8,128)(2,1)}, bf16[256,512]{1,0:T(8,128)(2,1)}) custom-call(bf16[256,1024]{1,0:T(8,128)(2,1)} %value_ref.1, bf16[256,1024]{1,0:T(8,128)(2,1)} %gate_ref.1, f32[31,1024]{1,0:T(8,128)} %taps_ref.1, f32[1,1024]{1,0:T(1,128)} %bitcast.9, f32[1,1024]{1,0:T(1,128)} %bitcast.10, f32[1,1024]{1,0:T(1,128)} %bitcast.11, ...), custom_call_target="tpu_custom_call" | custom-call | tf_op jit(solution)/shard_map/filter_and_experts/pallas_call | solution.py:357
  120.9 0.0 copy-start
  120.9 2.3 %copy.19 = bf16[256,2048]{1,0:T(8,128)(2,1)} copy(bf16[256,2048]{1,0:T(8,128)(2,1)} %get-tuple-element.4) | data formatting | bytes 2097152
  123.3 0.0 copy-done
  123.3 0.7 copy.20
Async XLA Ops:
  120.9 2.4 %copy-start = (bf16[256,512]{1,0:T(8,128)(2,1)S(1)}, bf16[256,512]{1,0:T(8,128)(2,1)}, u32[]{:S(2)}) copy-start(bf16[256,512]{1,0:T(8,128)(2,1)} %get-tuple-element.5) | copy-start | bytes 786436

commit v2 on v1

--- a/solution.py
+++ b/solution.py
@@ -23,7 +23,23 @@
 TOKENS = 256
 WIDTH = 512
 HALF = ROWS // 2
-ORDER = (0, 1, -2, 2, -3, 3, 4, -1)
+ORDER = (0, 2, -2, 4, 3, -3, 1, -1)
+DIRECT = tuple(by in (0, 1, -1) for by in ORDER)
+SCHEDULE = (
+    "F3 F2 F1 W0",
+    "C0 A1 A2 F0",
+    "P0 P1 P2 D0",
+    "P3 G0 B1 A3",
+    "B2 E0 C1 A4",
+    "A5 B3 C2 D1",
+    "B4 B5 C6 C3",
+    "C7 D2 E1 C4",
+    "C5 D6 D3 D7",
+    "E2 D4 D5 E6",
+    "E3 E7 E4 E5",
+)
+OPS = tuple(("ABCDEFPGW".index(word[0]), int(word[1:])) for line in SCHEDULE for word in line.split())
+GATHERED = NZ - sum(DIRECT)
 TAPS = 31
 CHANNELS = 1024
 TILE = 64
@@ -35,20 +51,31 @@
     )
 
 
-def travel(group):
-    value = jnp.int32(ORDER[0])
-    for index, by in enumerate(ORDER):
-        value = jnp.where(group == index, jnp.int32(by), value)
+def lookup(table, index):
+    value = jnp.int32(table[0])
+    for at, entry in enumerate(table):
+        if at and entry != table[0]:
+            value = jnp.where(index == at, jnp.int32(entry), value)
     return value
 
 
+def is_direct(group):
+    value = jnp.bool_(False)
+    for index, direct in enumerate(DIRECT):
+        if direct:
+            value = jnp.logical_or(value, group == index)
+    return value
+
+
 def kernel(
-    value_ref, gate_ref, taps_ref, fbias_ref, ngain_ref, nshift_ref, ow_hbm, obias_ref,
-    xin_ref, egain_ref, routes_ref, rweights_ref, wg_hbm, wu_hbm, wd_hbm,
+    value_hbm, gate_hbm, taps_hbm, fbias_hbm, ngain_hbm, nshift_hbm, ow_hbm, obias_hbm,
+    xin_hbm, egain_hbm, routes_hbm, rweights_hbm, wg_hbm, wu_hbm, wd_hbm,
     mixer_ref, out_ref,
+    value_ref, gate_ref, taps_ref, fbias_ref, ngain_ref, nshift_ref, obias_ref,
+    xin_ref, egain_ref, routes_ref, rweights_ref,
     rm, tk, pick, nb, outgoing, rows_in, wg, wu, wd, ow, parts, first_in, second_out, second_in,
     summed, ret, halo_out, halo_in, gbuf, filt, act,
-    load_sem, disp_send, disp_recv, ag_send, ag_recv, fwd_send, fwd_recv,
+    early_sem, load_sem, disp_send, disp_recv, ag_send, ag_recv, fwd_send, fwd_recv,
     rs1_send, rs1_recv, rs2_send, rs2_recv, ret_send, ret_recv, halo_send, halo_recv,
 ):
     me = lax.axis_index("ep")
@@ -59,6 +86,29 @@
     after = (line + 1) % (NEP * NTP)
     to_right, to_left = {"ep": me, "tp": right}, {"ep": me, "tp": left}
     to_after = {"ep": after // NTP, "tp": after % NTP}
+
+    early = [
+        pltpu.make_async_copy(src, dst, early_sem.at[index])
+        for index, (src, dst) in enumerate((
+            (routes_hbm, routes_ref), (rweights_hbm, rweights_ref), (xin_hbm, xin_ref), (egain_hbm, egain_ref),
+            (value_hbm, value_ref), (gate_hbm, gate_ref), (taps_hbm, taps_ref), (fbias_hbm, fbias_ref),
+            (ngain_hbm, ngain_ref), (nshift_hbm, nshift_ref), (obias_hbm, obias_ref),
+        ))
+    ]
+    for load in early:
+        load.start()
+
+    before = (line + NEP * NTP - 1) % (NEP * NTP)
+    barrier = pltpu.get_barrier_semaphore()
+
+    def greet(i, carry):
+        peer = {"ep": (me + i) % NEP, "tp": y}
+        pl.semaphore_signal(barrier, inc=1, device_id=peer, device_id_type=MESH)
+        return carry
+
+    lax.fori_loop(1, NEP, greet, 0)
+    for peer in (to_right, to_left, to_after, {"ep": before // NTP, "tp": before % NTP}):
+        pl.semaphore_signal(barrier, inc=1, device_id=peer, device_id_type=MESH)
 
     loads = []
     for k, shift in enumerate((0, 3, 1, 2)):
@@ -72,6 +122,8 @@
     for load in loads:
         load.start()
 
+    for load in early[:2]:
+        load.wait()
     routes = routes_ref[...]
     expert = lax.broadcasted_iota(I32, (NEP, TOKENS), 0)
     named0 = routes[0:1, :] == expert
@@ -86,15 +138,18 @@
         weight = jnp.broadcast_to(rweights_ref[k : k + 1, :], (NEP, TOKENS))
         tk[k] = jnp.concatenate([jnp.where(hit, rank, -1.0), weight], 0).T
 
-    columns = pl.ds(pl.multiple_of(y * WIDTH, WIDTH), WIDTH)
+    columns = [pl.ds(pl.multiple_of((y + shift) % NTP * WIDTH, WIDTH), WIDTH) for shift in (0, 3, 1, 2)]
 
     def normed(i, carry):
         at = pl.ds(pl.multiple_of(i * 16, 16), 16)
         tokens = xin_ref[at, :].astype(F32)
         scale = lax.rsqrt(jnp.mean(tokens * tokens, 1, keepdims=True) + EPS)
-        nb[at, :] = (xin_ref[at, columns].astype(F32) * scale * egain_ref[0:1, columns]).astype(BF16)
+        for k in range(NTP):
+            nb[k, at, :] = (xin_ref[at, columns[k]].astype(F32) * scale * egain_ref[0:1, columns[k]]).astype(BF16)
         return carry
 
+    for load in early[2:4]:
+        load.wait()
     lax.fori_loop(0, TOKENS // 16, normed, 0)
 
     row = lax.broadcasted_iota(I32, (ROWS, NEP), 0)
@@ -102,14 +157,19 @@
     slot_row = (lax.broadcasted_iota(I32, (ROWS, TOKENS), 0) % SLOTS).astype(F32)
 
     def place(group):
-        target = (z + travel(group) + NZ) % NZ
+        target = (z + lookup(ORDER, group) + NZ) % NZ
         spread = (row // SLOTS + target * PLANE == col).astype(F32).astype(BF16)
         ranks = jnp.dot(spread, rm[...], preferred_element_type=F32)
         chosen = (ranks == slot_row).astype(F32).astype(BF16)
-        outgoing[group] = jnp.dot(chosen, nb[...], preferred_element_type=F32).astype(BF16)
+        outgoing[0, group] = jnp.dot(chosen, nb[0], preferred_element_type=F32).astype(BF16)
+
+        @pl.when(is_direct(group))
+        def _():
+            for k in range(1, NTP):
+                outgoing[k, group] = jnp.dot(chosen, nb[k], preferred_element_type=F32).astype(BF16)
 
     def dispatch(group):
-        target = (z + travel(group) + NZ) % NZ
+        target = (z + lookup(ORDER, group) + NZ) % NZ
 
         def one(q, carry):
             index = (own + q) % PLANE
@@ -117,16 +177,24 @@
             at = pl.ds(pl.multiple_of(index * SLOTS, SLOTS), SLOTS)
             mine = pl.ds(pl.multiple_of(own * SLOTS, SLOTS), SLOTS)
 
-            @pl.when(there != me)
+            @pl.when(jnp.logical_not(is_direct(group)))
             def _():
                 copy_to(
-                    outgoing.at[group, at, :], rows_in.at[0, group, mine, :], disp_send, disp_recv.at[group],
-                    {"ep": there, "tp": y},
+                    outgoing.at[0, group, at, :], rows_in.at[0, group, mine, :],
+                    disp_send.at[group], disp_recv.at[group], {"ep": there, "tp": y},
                 ).start()
 
+            @pl.when(jnp.logical_and(is_direct(group), there != me))
+            def _():
+                copy_to(
+                    outgoing.at[:, group, at, :], rows_in.at[:, group, mine, :],
+                    disp_send.at[group], disp_recv.at[group], {"ep": there, "tp": y},
+                ).start()
+
             @pl.when(there == me)
             def _():
-                rows_in[0, group, mine, :] = outgoing[group, mine, :]
+                for k in range(NTP):
+                    rows_in[k, group, mine, :] = outgoing[k, group, mine, :]
 
             return carry
 
@@ -142,8 +210,6 @@
             dispatch(group - 1)
 
         return carry
-
-    lax.fori_loop(0, NZ + 1, place_and_send, 0)
 
     def gated(i, carry):
         at = pl.ds(pl.multiple_of(i * 16, 16), 16)
@@ -156,9 +222,15 @@
 
         return carry
 
-    lax.fori_loop(0, TOKENS // 16, gated, 0)
+    for load in early[4:]:
+        load.wait()
+    lax.fori_loop(TOKENS // 16 - 2, TOKENS // 16, gated, 0)
+    place(0)
+    pl.semaphore_wait(barrier, NEP - 1 + 4)
     halo = copy_to(halo_out, halo_in, halo_send, halo_recv, to_after)
     halo.start()
+    lax.fori_loop(1, NZ + 1, place_and_send, 0)
+    lax.fori_loop(0, TOKENS // 16 - 2, gated, 0)
 
     def conv(tile):
         def lanes(block, carry):
@@ -192,17 +264,19 @@
         out = jnp.dot(act[...], ow[:, at], preferred_element_type=F32) + obias_ref[0:1, at]
         mixer_ref[:, at] = out.astype(BF16)
 
+    def arrived(g):
+        for group, by in enumerate(ORDER):
+            every = rows_in.at[0, group]
+            if DIRECT[group]:
+                count = ROWS - SLOTS if by == 0 else ROWS
+                every = rows_in.at[:, group, pl.ds(0, count), :]
+
+            @pl.when(g == group)
+            def _():
+                copy_to(every, every, disp_send.at[group], disp_recv.at[group], to_right).wait_recv()
+
     def gather_own(g):
-        @pl.when(g == 0)
-        def _():
-            some = rows_in.at[0, 0, pl.ds(0, ROWS - SLOTS), :]
-            copy_to(some, some, disp_send, disp_recv.at[0], to_right).wait_recv()
-
-        @pl.when(g > 0)
-        def _():
-            every = rows_in.at[0, g]
-            copy_to(every, every, disp_send, disp_recv.at[g], to_right).wait_recv()
-
+        arrived(g)
         copy_to(rows_in.at[0, g], rows_in.at[1, g], ag_send, ag_recv.at[0, g], to_right).start()
         copy_to(rows_in.at[0, g], rows_in.at[2, g], ag_send, ag_recv.at[1, g], to_left).start()
 
@@ -216,7 +290,15 @@
 
     def experts(g):
         whole = rows_in.at[3, g]
-        copy_to(whole, whole, fwd_send, fwd_recv.at[g], to_right).wait_recv()
+
+        @pl.when(is_direct(g))
+        def _():
+            arrived(g)
+
+        @pl.when(jnp.logical_not(is_direct(g)))
+        def _():
+            copy_to(whole, whole, fwd_send, fwd_recv.at[g], to_right).wait_recv()
+
         gate_pre = jnp.zeros((ROWS, WIDTH), F32)
         up_pre = jnp.zeros((ROWS, WIDTH), F32)
         for k in range(NTP):
@@ -250,7 +332,7 @@
         copy_to(second_out.at[1, g], second_in.at[1, g], rs2_send, rs2_recv.at[1, g], to_left).wait_recv()
         total = parts[0, g].astype(F32) + second_in[0, g].astype(F32) + second_in[1, g].astype(F32)
         summed[g] = total.astype(BF16)
-        source = (z - travel(g) + NZ) % NZ
+        source = (z - lookup(ORDER, g) + NZ) % NZ
         mine = pl.ds(pl.multiple_of(me * SLOTS, SLOTS), SLOTS)
 
         def one(q, carry):
@@ -272,7 +354,7 @@
 
         lax.fori_loop(0, PLANE, one, 0)
 
-    def picks():
+    def picks(_):
         lane = lax.broadcasted_iota(I32, (NEP, NEP * SLOTS), 1)
         spread = (lane // SLOTS == lax.broadcasted_iota(I32, (NEP, NEP * SLOTS), 0)).astype(F32).astype(BF16)
         slot = (lax.broadcasted_iota(I32, (TOKENS, NEP * SLOTS), 1) % SLOTS).astype(F32)
@@ -280,56 +362,39 @@
             ranks = jnp.dot(tk[k][:, 0:NEP].astype(BF16), spread, preferred_element_type=F32)
             pick[k] = (ranks == slot).astype(F32).astype(BF16)
 
-    def step(t, carry):
-        @pl.when(t < NZ)
-        def _():
-            gather_own(t)
-
-        @pl.when(jnp.logical_and(t >= 1, t < NZ + 1))
-        def _():
-            gather_on(t - 1)
-
-        @pl.when(t >= 4)
-        def _():
-            send_back(t - 4)
-
-        @pl.when(jnp.logical_and(t >= 3, t < NZ + 3))
-        def _():
-            reduce_on(t - 3)
-
-        @pl.when(t == 2)
-        def _():
-            for load in loads[:12]:
-                load.wait()
-
-        @pl.when(jnp.logical_and(t >= 2, t < NZ + 2))
-        def _():
-            experts(t - 2)
-
-        @pl.when(t == 0)
+    def loaded(_):
+        for load in loads[:12]:
+            load.wait()
+
+    def filtered(tile):
+        @pl.when(tile == 0)
         def _():
             halo.wait()
             gbuf[0:32, :] = jnp.where(line == 0, 0.0, halo_in[...].astype(F32))
 
-        @pl.when(t < 4)
-        def _():
-            conv(t)
-
-        @pl.when(t == 4)
+        conv(tile)
+
+    def projected(chunk):
+        @pl.when(chunk == 0)
         def _():
             loads[12].wait()
 
-        @pl.when(jnp.logical_and(t >= 4, t < 8))
-        def _():
-            project(t - 4)
-
-        @pl.when(t == 8)
-        def _():
-            picks()
+        project(chunk)
+
+    actions = (gather_own, gather_on, experts, reduce_on, send_back, filtered, projected, picks, loaded)
+
+    def step(i, carry):
+        code = lookup([op for op, _ in OPS], i)
+        which = lookup([index for _, index in OPS], i)
+        for number, action in enumerate(actions):
+
+            @pl.when(code == number)
+            def _():
+                action(which)
 
         return carry
 
-    lax.fori_loop(0, NZ + 4, step, 0)
+    lax.fori_loop(0, len(OPS), step, 0)
 
     but_one = ret.at[pl.ds(0, (NEP - 1) * SLOTS), :]
     copy_to(but_one, but_one, ret_send, ret_recv, to_right).wait_recv()
@@ -339,11 +404,17 @@
         expert_out = expert_out + picked * tk[k][:, NEP : NEP + 1]
     out_ref[...] = expert_out.astype(BF16)
 
-    copy_to(but_one, but_one, disp_send, ret_recv, to_right).wait_send()
+    for group, by in enumerate(ORDER):
+        every = rows_in.at[0, group]
+        if DIRECT[group]:
+            every = rows_in.at[:, group, pl.ds(0, ROWS - SLOTS if by == 0 else ROWS), :]
+        copy_to(every, every, disp_send.at[group], ret_recv, to_right).wait_send()
     copy_to(but_one, but_one, ret_send, ret_recv, to_right).wait_send()
-    copy_to(second_in, second_in, ag_send, ret_recv, to_right).wait_send()
+    some = second_in.at[:, pl.ds(0, GATHERED)]
+    copy_to(some, some, ag_send, ret_recv, to_right).wait_send()
     copy_to(second_in, second_in, rs2_send, ret_recv, to_right).wait_send()
-    copy_to(first_in, first_in, fwd_send, ret_recv, to_right).wait_send()
+    some = first_in.at[:, pl.ds(0, GATHERED)]
+    copy_to(some, some, fwd_send, ret_recv, to_right).wait_send()
     copy_to(first_in, first_in, rs1_send, ret_recv, to_right).wait_send()
 
 
@@ -352,22 +423,29 @@
     expert_input, expert_gain, route_experts, route_weights, gate_weights, up_weights, down_weights,
 ):
     vmem = pl.BlockSpec(memory_space=pltpu.VMEM)
-    hbm = pl.BlockSpec(memory_space=pl.ANY)
+    hbm = pl.BlockSpec(memory_space=pltpu.HBM)
     dma = pltpu.SemaphoreType.DMA
+    arguments = (
+        filter_value, filter_gate, filter_taps, filter_bias[None], norm_gain[None], norm_shift[None],
+        out_weight, out_bias[None], expert_input, expert_gain[None], route_experts.T, route_weights.T,
+        gate_weights, up_weights, down_weights,
+    )
+    small = [argument for index, argument in enumerate(arguments[:12]) if index != 6]
     return pl.pallas_call(
         kernel,
         out_shape=(
             jax.ShapeDtypeStruct((TOKENS, 2048), BF16),
             jax.ShapeDtypeStruct((TOKENS, WIDTH), BF16),
         ),
-        in_specs=[vmem] * 6 + [hbm] + [vmem] * 5 + [hbm] * 3,
+        in_specs=[hbm] * len(arguments),
         out_specs=(vmem, vmem),
-        scratch_shapes=[
+        scratch_shapes=[pltpu.VMEM(argument.shape, argument.dtype) for argument in small]
+        + [
             pltpu.VMEM((NEP, TOKENS), BF16),
             pltpu.VMEM((2, TOKENS, 2 * NEP), F32),
             pltpu.VMEM((2, TOKENS, NEP * SLOTS), BF16),
-            pltpu.VMEM((TOKENS, WIDTH), BF16),
-            pltpu.VMEM((NZ, ROWS, WIDTH), BF16),
+            pltpu.VMEM((NTP, TOKENS, WIDTH), BF16),
+            pltpu.VMEM((NTP, NZ, ROWS, WIDTH), BF16),
             pltpu.VMEM((NTP, NZ, ROWS, WIDTH), BF16),
             pltpu.VMEM((NTP, WIDTH, WIDTH), BF16),
             pltpu.VMEM((NTP, WIDTH, WIDTH), BF16),
@@ -384,17 +462,13 @@
             pltpu.VMEM((TOKENS + 32, CHANNELS), F32),
             pltpu.VMEM((TILE, CHANNELS), F32),
             pltpu.VMEM((TOKENS, CHANNELS), BF16),
-            dma((13,)),
-            dma, dma((NZ,)), dma, dma((2, NZ)), dma, dma((NZ,)),
+            dma((11,)), dma((13,)),
+            dma((NZ,)), dma((NZ,)), dma, dma((2, NZ)), dma, dma((NZ,)),
             dma, dma((2, NZ)), dma, dma((2, NZ)), dma, dma, dma, dma,
         ],
-        compiler_params=pltpu.CompilerParams(has_side_effects=True, vmem_limit_bytes=56 * 1024 * 1024),
+        compiler_params=pltpu.CompilerParams(collective_id=0, has_side_effects=True, vmem_limit_bytes=46 * 1024 * 1024),
         name="filter_and_experts",
-    )(
-        filter_value, filter_gate, filter_taps, filter_bias[None], norm_gain[None], norm_shift[None],
-        out_weight, out_bias[None], expert_input, expert_gain[None], route_experts.T, route_weights.T,
-        gate_weights, up_weights, down_weights,
-    )
+    )(*(pltpu.with_memory_space_constraint(argument, pltpu.HBM) for argument in arguments))
 
 
 def solution(mesh):

time: 124 us -> 96.5 us (0.78)
  Pallas kernels: 120 us -> 94 us
  local copies, waits for them, and re-layouts: 3.05 us -> 1.67 us
    pallas_call x1, Pallas kernels: 120 us -> 94 us  [local(): pl.pallas_call(kernel, out_shape=(jax.ShapeDtypeStruct((TOKENS, 2048), BF...]
    unnamed x4 -> x2, local copies, waits for them, and re-layouts: 3.05 us -> 1.67 us
where the time goes in v2:
time: 96.5 us; the launch traced here: 96.3 us
  Pallas kernels  94 us (97%)
  local copies, waits for them, and re-layouts  1.67 us (2%)
    pallas_call x1, Pallas kernels, local(): pl.pallas_call(kernel, out_shape=(jax.ShapeDtypeStruct((TOKENS, 2048), BF...  94 us

profile of v2, /device:TPU:1, one launch (start us, length us, event | category | flops | bytes accessed | tf_op | source)
XLA Modules:
  0.0 96.3 jit_solution(5124762009635854318)
XLA Ops:
  0.6 94.0 %filter_and_experts.1 = (bf16[256,2048]{1,0:T(8,128)(2,1)S(1)}, bf16[256,512]{1,0:T(8,128)(2,1)S(1)}) custom-call(bf16[256,1024]{1,0:T(8,128)(2,1)} %value_hbm.1, bf16[256,1024]{1,0:T(8,128)(2,1)} %gate_hbm.1, f32[31,1024]{1,0:T(8,128)} %taps_hbm.1, f32[1,1024]{1,0:T(1,128)} %bitcast.9, f32[1,1024]{1,0:T(1,128)} %bitcast.10, f32[1,1024]{1,0:T(1,128)} %bitcast.11, ...), custom_call_target="tpu_custom_call" | custom-call | tf_op jit(solution)/shard_map/filter_and_experts/pallas_call | solution.py:434
  94.7 1.0 %copy.19 = bf16[256,2048]{1,0:T(8,128)(2,1)} copy(bf16[256,2048]{1,0:T(8,128)(2,1)S(1)} %get-tuple-element.4) | data formatting | bytes 2097152
  95.6 0.7 copy.20

commit v3 on v2

v3 whole, which is shorter than its diff:
```python
import functools

import jax
import jax.numpy as jnp
from jax import lax
from jax.experimental import pallas as pl
from jax.experimental.pallas import tpu as pltpu
from jax.sharding import PartitionSpec as P

MESH = pl.DeviceIdType.MESH
BF16, F32, I32 = jnp.bfloat16, jnp.float32, jnp.int32

EPS = 1e-06
LIMIT = 7.0
ALPHA = 1.702

NZ = 8
NX = 4
PLANE = 8
NEP = 64
NTP = 4
SLOTS = 16
PLANE_ROWS = PLANE * SLOTS
TOKENS = 256
WIDTH = 512
AWAY = (0, 1, -1, 2, -2, 3, -3, 4)
DIRECT = (
    1, 2, 3, 4, 5, 6, 8,
)
SCHEDULE = (
    "S9 S11 S0 S1",
    "S12 F3 S10 F2",
    "F1 S13 A0 F0",
    "S14 A9 P0 P1",
    "P2 B0 A11 S7",
    "P3 G0 B9 A12",
    "W0 C0 S15 B11",
    "A10 S5 S3 B12",
    "A13 D0 A7 B10",
    "A14 S8 S6 B13",
    "A15 E0 B7 C5",
    "B14 C6 B15 D5",
    "S4 S2 R0 D6",
    "C7 E5 C4 C3",
    "E6 D7 D4 C2",
    "C1 D3 E7 E4",
    "D2 D1 R5 E3",
    "R6 E2 E1 R7",
    "R4 R3 R2 R1",
)
KINDS = "SABDERCFPGW"
STEPS = tuple(KINDS.index(word[0]) * 16 + int(word[1:]) for line in SCHEDULE for word in line.split())
WORDS = tuple(
    sum(step << 8 * at for at, step in enumerate(STEPS[first : first + 3])) for first in range(0, len(STEPS), 3)
)
ROWS = PLANE_ROWS
PART = ROWS // 2
QUARTER = PART // 2
IS_DIRECT = tuple(int(half in DIRECT) for half in range(2 * NZ))
GATHERED = 2 * NZ - len(DIRECT)
TAPS = 31
CHANNELS = 1024
TILE = 64


def copy_to(src, dst, send, recv, device):
    return pltpu.make_async_remote_copy(
        src_ref=src, dst_ref=dst, send_sem=send, recv_sem=recv, device_id=device, device_id_type=MESH
    )


def lookup(table, index):
    value = jnp.int32(table[0])
    for at, entry in enumerate(table):
        if at and entry != table[0]:
            value = jnp.where(index == at, jnp.int32(entry), value)
    return value


def is_direct(half):
    return lookup(IS_DIRECT, half) == 1


def kernel(
    value_hbm, gate_hbm, taps_hbm, fbias_hbm, ngain_hbm, nshift_hbm, ow_hbm, obias_hbm,
    xin_hbm, egain_hbm, routes_hbm, rweights_hbm, wg_hbm, wu_hbm, wd_hbm,
    mixer_ref, out_ref,
    value_ref, gate_ref, taps_ref, fbias_ref, ngain_ref, nshift_ref, obias_ref,
    xin_ref, egain_ref, routes_ref, rweights_ref,
    rm, tk, pick, nb, outgoing, rows_in, wg, wu, wd, ow, parts, first_in, second_out, second_in,
    summed, ret, total, halo_out, halo_in, gbuf, filt, act,
    early_sem, load_sem, disp_send, disp_recv, ag_send, ag_recv, fwd_send, fwd_recv,
    rs1_send, rs1_recv, rs2_send, rs2_recv, ret_send, ret_recv, halo_send, halo_recv,
):
    me = lax.axis_index("ep")
    y = lax.axis_index("tp")
    z, x, core = me // PLANE, me % PLANE // 2, me % 2
    right, left = (y + 1) % NTP, (y + NTP - 1) % NTP
    line = me * NTP + y
    after = (line + 1) % (NEP * NTP)
    to_right, to_left = {"ep": me, "tp": right}, {"ep": me, "tp": left}
    to_after = {"ep": after // NTP, "tp": after % NTP}

    early = [
        pltpu.make_async_copy(src, dst, early_sem.at[index])
        for index, (src, dst) in enumerate((
            (routes_hbm, routes_ref), (rweights_hbm, rweights_ref), (xin_hbm, xin_ref), (egain_hbm, egain_ref),
            (value_hbm, value_ref), (gate_hbm, gate_ref), (taps_hbm, taps_ref), (fbias_hbm, fbias_ref),
            (ngain_hbm, ngain_ref), (nshift_hbm, nshift_ref), (obias_hbm, obias_ref),
        ))
    ]
    for load in early[:4]:
        load.start()

    before = (line + NEP * NTP - 1) % (NEP * NTP)
    barrier = pltpu.get_barrier_semaphore()

    def greet(i, carry):
        peer = {"ep": (me + NEP // 2 + i) % NEP, "tp": y}
        pl.semaphore_signal(barrier, inc=1, device_id=peer, device_id_type=MESH)
        return carry

    lax.fori_loop(0, NEP // 2, greet, 0)
    lax.fori_loop(NEP // 2 + 1, NEP, greet, 0)
    for peer in (to_right, to_left, to_after, {"ep": before // NTP, "tp": before % NTP}):
        pl.semaphore_signal(barrier, inc=1, device_id=peer, device_id_type=MESH)

    for load in early[4:]:
        load.start()
    loads = []
    for k, shift in enumerate((0, 3, 1, 2)):
        at = pl.ds(pl.multiple_of((y + shift) % NTP * WIDTH, WIDTH), WIDTH)
        loads.append(pltpu.make_async_copy(wg_hbm.at[0, at, :], wg.at[k], load_sem.at[k]))
        loads.append(pltpu.make_async_copy(wu_hbm.at[0, at, :], wu.at[k], load_sem.at[4 + k]))
    for k, shift in enumerate((0, 1, 3, 2)):
        at = pl.ds(pl.multiple_of((y + shift) % NTP * WIDTH, WIDTH), WIDTH)
        loads.append(pltpu.make_async_copy(wd_hbm.at[0, :, at], wd.at[k], load_sem.at[8 + k]))
    loads.append(pltpu.make_async_copy(ow_hbm, ow, load_sem.at[12]))
    for load in loads:
        load.start()

    for load in early[:2]:
        load.wait()
    routes = routes_ref[...]
    expert = lax.broadcasted_iota(I32, (NEP, TOKENS), 0)
    named0 = routes[0:1, :] == expert
    named1 = routes[1:2, :] == expert
    named = jnp.logical_or(named0, named1)
    earlier = (
        lax.broadcasted_iota(I32, (TOKENS, TOKENS), 0) < lax.broadcasted_iota(I32, (TOKENS, TOKENS), 1)
    ).astype(F32).astype(BF16)
    rank = jnp.dot(named.astype(F32).astype(BF16), earlier, preferred_element_type=F32)
    rm[...] = jnp.where(named, rank, -1.0).astype(BF16)
    for k, hit in enumerate((named0, named1)):
        weight = jnp.broadcast_to(rweights_ref[k : k + 1, :], (NEP, TOKENS))
        tk[k] = jnp.concatenate([jnp.where(hit, rank, -1.0), weight], 0).T

    columns = [pl.ds(pl.multiple_of((y + shift) % NTP * WIDTH, WIDTH), WIDTH) for shift in (0, 3, 1, 2)]

    def normed(i, carry):
        at = pl.ds(pl.multiple_of(i * 16, 16), 16)
        tokens = xin_ref[at, :].astype(F32)
        scale = lax.rsqrt(jnp.mean(tokens * tokens, 1, keepdims=True) + EPS)
        for k in range(NTP):
            nb[k, at, :] = (xin_ref[at, columns[k]].astype(F32) * scale * egain_ref[0:1, columns[k]]).astype(BF16)
        return carry

    for load in early[2:4]:
        load.wait()
    lax.fori_loop(0, TOKENS // 16, normed, 0, unroll=4)

    row = lax.broadcasted_iota(I32, (PLANE_ROWS, NEP), 0)
    col = lax.broadcasted_iota(I32, (PLANE_ROWS, NEP), 1)
    slot_row = (lax.broadcasted_iota(I32, (PLANE_ROWS, TOKENS), 0) % SLOTS).astype(F32)

    def ahead(r):
        return (z + lookup(AWAY, r) + NZ) % NZ

    def place(r):
        spread = (row // SLOTS + ahead(r) * PLANE == col).astype(F32).astype(BF16)
        ranks = jnp.dot(spread, rm[...], preferred_element_type=F32)
        chosen = (ranks == slot_row).astype(F32).astype(BF16)
        for k in range(NTP if IS_DIRECT[2 * r] or IS_DIRECT[2 * r + 1] else 1):
            outgoing[k, r] = jnp.dot(chosen, nb[k], preferred_element_type=F32).astype(BF16)

    def dispatch(half):
        r, part = half // 2, half % 2
        direct = is_direct(half)
        for i in range(4):
            target = (x + part + 2 * (i // 2)) % NX * 2 + i % 2
            there = ahead(r) * PLANE + target
            at = pl.ds(pl.multiple_of(target * SLOTS, SLOTS), SLOTS)
            mine = pl.ds(pl.multiple_of(part * PART + (i // 2 * 2 + core) * SLOTS, SLOTS), SLOTS)

            @pl.when(jnp.logical_and(jnp.logical_not(direct), there != me))
            def _():
                copy_to(
                    outgoing.at[0, r, at, :], rows_in.at[0, r, mine, :],
                    disp_send.at[half], disp_recv.at[half], {"ep": there, "tp": y},
                ).start()

            @pl.when(jnp.logical_and(direct, there != me))
            def _():
                copy_to(
                    outgoing.at[:, r, at, :], rows_in.at[:, r, mine, :],
                    disp_send.at[half], disp_recv.at[half], {"ep": there, "tp": y},
                ).start()

            if i < 2:

                @pl.when(there == me)
                def _():
                    for k in range(NTP if IS_DIRECT[0] else 1):
                        rows_in[k, 0, mine, :] = outgoing[k, 0, at, :]

    def gated(i, carry):
        at = pl.ds(pl.multiple_of(i * 16, 16), 16)
        product = (value_ref[at, :].astype(F32) * jax.nn.sigmoid(gate_ref[at, :].astype(F32))).astype(BF16)
        gbuf[pl.ds(pl.multiple_of(i * 16 + 32, 16), 16), :] = product.astype(F32)

        @pl.when(i >= TOKENS // 16 - 2)
        def _():
            halo_out[pl.ds(pl.multiple_of(i * 16 - (TOKENS - 32), 16), 16), :] = product

        return carry

    for load in early[4:]:
        load.wait()
    lax.fori_loop(0, TOKENS // 16, gated, 0)
    for r in range(NZ):
        place(r)
    pl.semaphore_wait(barrier, NEP - 1 + 4)
    halo = copy_to(halo_out, halo_in, halo_send, halo_recv, to_after)
    halo.start()

    def conv(tile):
        def lanes(block, carry):
            at = pl.ds(pl.multiple_of(block * 128, 128), 128)
            window = gbuf[pl.ds(pl.multiple_of(tile * TILE, TILE), TILE + 32), at]
            value = jnp.broadcast_to(fbias_ref[0:1, at], (TILE, 128))
            for r in range(8):
                moved = window if r == 0 else pltpu.roll(window, TILE + 32 - r, 0)
                for q in range(5):
                    j = 8 * q + r - 2
                    if 0 <= j < TAPS:
                        value = value + taps_ref[j : j + 1, at] * moved[8 * q : 8 * q + TILE]
            filt[:, at] = value
            return carry

        lax.fori_loop(0, CHANNELS // 128, lanes, 0)

        def norm(i, carry):
            at = pl.ds(pl.multiple_of(i * 16, 16), 16)
            rows = filt[at, :]
            centred = rows - jnp.mean(rows, 1, keepdims=True)
            variance = jnp.mean(centred * centred, 1, keepdims=True)
            out = centred * lax.rsqrt(variance + EPS) * ngain_ref[0:1, :] + nshift_ref[0:1, :]
            act[pl.ds(pl.multiple_of(tile * TILE + i * 16, 16), 16), :] = (out * jax.nn.sigmoid(out)).astype(BF16)
            return carry

        lax.fori_loop(0, TILE // 16, norm, 0, unroll=True)

    def project(chunk):
        at = pl.ds(pl.multiple_of(chunk * 512, 512), 512)
        out = jnp.dot(act[...], ow[:, at], preferred_element_type=F32) + obias_ref[0:1, at]
        mixer_ref[:, at] = out.astype(BF16)

    def rows_of(half):
        return pl.ds(pl.multiple_of(half % 2 * PART, PART), PART)

    def arrived(half):
        r, direct, other = half // 2, is_direct(half), half != 0

        @pl.when(jnp.logical_and(jnp.logical_not(direct), other))
        def _():
            every = rows_in.at[0, r, rows_of(half), :]
            copy_to(every, every, disp_send.at[half], disp_recv.at[half], to_right).wait_recv()

        @pl.when(jnp.logical_and(direct, other))
        def _():
            every = rows_in.at[:, r, rows_of(half), :]
            copy_to(every, every, disp_send.at[half], disp_recv.at[half], to_right).wait_recv()

        @pl.when(half == 0)
        def _():
            copy_to(sent(0), sent(0), disp_send.at[0], disp_recv.at[0], to_right).wait_recv()

    def sent(half):
        rows = pl.ds(0, PART if half else PART - SLOTS)
        return rows_in.at[:, half // 2, rows, :] if IS_DIRECT[half] else rows_in.at[0, half // 2, rows, :]

    def to_next(half, block, device, side):
        r, at = half // 2, rows_of(half)
        return copy_to(
            rows_in.at[0, r, at, :], rows_in.at[block, r, at, :], ag_send, ag_recv.at[side, half], device
        )

    def gather_own(half):
        arrived(half)
        to_next(half, 1, to_right, 0).start()
        to_next(half, 2, to_left, 1).start()

    def gather_on(half):
        r, start = half // 2, half % 2 * PART
        for block, device, side in ((1, to_right, 0), (2, to_left, 1)):
            at = pl.ds(pl.multiple_of(start + side * QUARTER, QUARTER), QUARTER)
            to_next(half, block, device, side).wait_recv()
            copy_to(
                rows_in.at[block, r, at, :], rows_in.at[3, r, at, :], fwd_send, fwd_recv.at[half], device
            ).start()

    top, low = pl.ds(0, PART), pl.ds(PART, PART)

    def first_hop(r, side):
        at, device = ((top, to_right), (low, to_left))[side]
        return copy_to(parts.at[3, r, at, :], first_in.at[side * NZ + r], rs1_send, rs1_recv.at[side, r], device)

    def second_hop(r, side):
        device = (to_right, to_left)[side]
        return copy_to(second_out.at[side, r], second_in.at[side * NZ + r], rs2_send, rs2_recv.at[side, r], device)

    def experts(r):
        for part in range(2):
            half = 2 * r + part
            whole = rows_in.at[3, r, pl.ds(part * PART, PART), :]
            direct = is_direct(half)

            @pl.when(direct)
            def _():
                arrived(half)

            @pl.when(jnp.logical_not(direct))
            def _():
                copy_to(whole, whole, fwd_send, fwd_recv.at[half], to_right).wait_recv()

        gate_pre = jnp.zeros((ROWS, WIDTH), F32)
        up_pre = jnp.zeros((ROWS, WIDTH), F32)
        for k in range(NTP):
            block = rows_in[k, r]
            gate_pre = gate_pre + jnp.dot(block, wg[k], preferred_element_type=F32)
            up_pre = up_pre + jnp.dot(block, wu[k], preferred_element_type=F32)
        gate_held = jnp.minimum(gate_pre, LIMIT)
        up_held = jnp.clip(up_pre, -LIMIT, LIMIT)
        hidden = (gate_held * jax.nn.sigmoid(ALPHA * gate_held) * (up_held + 1.0)).astype(BF16)
        for k in (3, 1, 2, 0):
            parts[k, r] = jnp.dot(hidden, wd[k], preferred_element_type=F32).astype(BF16)
        first_hop(r, 0).start()
        first_hop(r, 1).start()

    def reduce_on(r):
        for side, (summing, plain) in enumerate(((top, low), (low, top))):
            first_hop(r, side).wait_recv()
            second_out[side, r, summing, :] = (
                parts[1 + side, r, summing, :].astype(F32) + first_in[side * NZ + r].astype(F32)
            ).astype(BF16)
            second_out[side, r, plain, :] = parts[1 + side, r, plain, :]
            second_hop(r, side).start()

    def send_back(r):
        second_hop(r, 0).wait_recv()
        second_hop(r, 1).wait_recv()
        reduced = parts[0, r].astype(F32) + second_in[r].astype(F32) + second_in[NZ + r].astype(F32)
        summed[r] = reduced.astype(BF16)
        source = (z - lookup(AWAY, r) + NZ) % NZ
        mine = pl.ds(pl.multiple_of(me * SLOTS, SLOTS), SLOTS)
        for i in range(8):
            there = source * PLANE + (x - i // 4 - 2 * (i % 4 // 2) + NX) % NX * 2 + i % 2
            at = pl.ds(i * SLOTS, SLOTS)

            @pl.when(there != me)
            def _():
                copy_to(
                    summed.at[r, at, :], ret.at[mine, :], ret_send, ret_recv.at[r], {"ep": there, "tp": y}
                ).start()

            if i < 2:

                @pl.when(there == me)
                def _():
                    ret[mine, :] = summed[r, at, :]

    def combine(r):
        for index in range(2):

            @pl.when((r == 0) == (index == 0))
            def _():
                every = ret.at[pl.ds(0, PLANE_ROWS - SLOTS if index == 0 else PLANE_ROWS), :]
                copy_to(every, every, ret_send, ret_recv.at[r], to_right).wait_recv()

        at = pl.ds(pl.multiple_of(ahead(r) * PLANE_ROWS, PLANE_ROWS), PLANE_ROWS)
        back = ret[at, :]
        for k in range(2):
            picked = jnp.dot(pick[k, :, at], back, preferred_element_type=F32)
            total[...] += picked * tk[k, :, NEP : NEP + 1]

    def picks(_):
        lane = lax.broadcasted_iota(I32, (NEP, NEP * SLOTS), 1)
        spread = (lane // SLOTS == lax.broadcasted_iota(I32, (NEP, NEP * SLOTS), 0)).astype(F32).astype(BF16)
        slot = (lax.broadcasted_iota(I32, (TOKENS, NEP * SLOTS), 1) % SLOTS).astype(F32)
        for k in range(2):
            ranks = jnp.dot(tk[k, :, 0:NEP].astype(BF16), spread, preferred_element_type=F32)
            pick[k] = (ranks == slot).astype(F32).astype(BF16)
        total[...] = jnp.zeros_like(total)

    def loaded(_):
        for load in loads[:12]:
            load.wait()

    def filtered(tile):
        @pl.when(tile == 0)
        def _():
            halo.wait()
            gbuf[0:32, :] = jnp.where(line == 0, 0.0, halo_in[...].astype(F32))

        conv(tile)

    def projected(chunk):
        @pl.when(chunk == 0)
        def _():
            loads[12].wait()

        project(chunk)

    actions = (
        dispatch, gather_own, gather_on, reduce_on, send_back, combine, experts, filtered, projected, picks, loaded,
    )

    def step(i, carry):
        place_in = i % 3
        shift = jnp.where(place_in == 0, jnp.int32(1), jnp.where(place_in == 1, jnp.int32(256), jnp.int32(65536)))
        code = lookup(WORDS, i // 3) // shift % 256
        kind, which = code // 16, code % 16
        for first, last in ((0, 3), (3, 7), (7, 11)):

            @pl.when(jnp.logical_and(kind >= first, kind < last))
            def _():
                for number in range(first, last):

                    @pl.when(kind == number)
                    def _():
                        actions[number](which)

        return carry

    lax.fori_loop(0, len(STEPS), step, 0)

    out_ref[...] = total[...].astype(BF16)

    for half in range(2 * NZ):
        copy_to(sent(half), sent(half), disp_send.at[half], disp_recv.at[half], to_right).wait_send()
    but_one = ret.at[pl.ds(0, (NEP - 1) * SLOTS), :]
    copy_to(but_one, but_one, ret_send, ret_recv.at[0], to_right).wait_send()
    some = second_in.at[pl.ds(0, GATHERED)]
    copy_to(some, some, ag_send, ret_recv.at[0], to_right).wait_send()
    copy_to(second_in, second_in, rs2_send, ret_recv.at[0], to_right).wait_send()
    some = first_in.at[pl.ds(0, GATHERED)]
    copy_to(some, some, fwd_send, ret_recv.at[0], to_right).wait_send()
    copy_to(first_in, first_in, rs1_send, ret_recv.at[0], to_right).wait_send()


def local(
    filter_value, filter_gate, filter_taps, filter_bias, norm_gain, norm_shift, out_weight, out_bias,
    expert_input, expert_gain, route_experts, route_weights, gate_weights, up_weights, down_weights,
):
    vmem = pl.BlockSpec(memory_space=pltpu.VMEM)
    hbm = pl.BlockSpec(memory_space=pltpu.HBM)
    dma = pltpu.SemaphoreType.DMA
    arguments = (
        filter_value, filter_gate, filter_taps, filter_bias[None], norm_gain[None], norm_shift[None],
        out_weight, out_bias[None], expert_input, expert_gain[None], route_experts.T, route_weights.T,
        gate_weights, up_weights, down_weights,
    )
    small = [argument for index, argument in enumerate(arguments[:12]) if index != 6]
    return pl.pallas_call(
        kernel,
        out_shape=(
            jax.ShapeDtypeStruct((TOKENS, 2048), BF16),
            jax.ShapeDtypeStruct((TOKENS, WIDTH), BF16),
        ),
        in_specs=[hbm] * len(arguments),
        out_specs=(vmem, vmem),
        scratch_shapes=[pltpu.VMEM(argument.shape, argument.dtype) for argument in small]
        + [
            pltpu.VMEM((NEP, TOKENS), BF16),
            pltpu.VMEM((2, TOKENS, 2 * NEP), F32),
            pltpu.VMEM((2, TOKENS, NEP * SLOTS), BF16),
            pltpu.VMEM((NTP, TOKENS, WIDTH), BF16),
            pltpu.VMEM((NTP, NZ, PLANE_ROWS, WIDTH), BF16),
            pltpu.VMEM((NTP, NZ, ROWS, WIDTH), BF16),
            pltpu.VMEM((NTP, WIDTH, WIDTH), BF16),
            pltpu.VMEM((NTP, WIDTH, WIDTH), BF16),
            pltpu.VMEM((NTP, WIDTH, WIDTH), BF16),
            pltpu.VMEM((CHANNELS, 2048), BF16),
            pltpu.VMEM((NTP, NZ, ROWS, WIDTH), BF16),
            pltpu.VMEM((2 * NZ, PART, WIDTH), BF16),
            pltpu.VMEM((2, NZ, ROWS, WIDTH), BF16),
            pltpu.VMEM((2 * NZ, ROWS, WIDTH), BF16),
            pltpu.VMEM((NZ, ROWS, WIDTH), BF16),
            pltpu.VMEM((NEP * SLOTS, WIDTH), BF16),
            pltpu.VMEM((TOKENS, WIDTH), F32),
            pltpu.VMEM((32, CHANNELS), BF16),
            pltpu.VMEM((32, CHANNELS), BF16),
            pltpu.VMEM((TOKENS + 32, CHANNELS), F32),
            pltpu.VMEM((TILE, CHANNELS), F32),
            pltpu.VMEM((TOKENS, CHANNELS), BF16),
            dma((11,)), dma((13,)),
            dma((2 * NZ,)), dma((2 * NZ,)), dma, dma((2, 2 * NZ)), dma, dma((2 * NZ,)),
            dma, dma((2, NZ)), dma, dma((2, NZ)), dma, dma((NZ,)), dma, dma,
        ],
        compiler_params=pltpu.CompilerParams(collective_id=0, has_side_effects=True, vmem_limit_bytes=46 * 1024 * 1024),
        name="filter_and_experts",
    )(*(pltpu.with_memory_space_constraint(argument, pltpu.HBM) for argument in arguments))


def solution(mesh):
    in_specs = (
        P(("ep", "tp"), None),
        P(("ep", "tp"), None),
        P(),
        P(),
        P(),
        P(),
        P(),
        P(),
        P("ep", None),
        P(),
        P("ep", None),
        P("ep", None),
        P("ep", None, "tp"),
        P("ep", None, "tp"),
        P("ep", "tp", None),
    )
    out_specs = (P(("ep", "tp"), None), P("ep", "tp"))
    return jax.shard_map(local, mesh=mesh, in_specs=in_specs, out_specs=out_specs, check_vma=False)
```

time: 96.5 us -> 88 us (0.912)
  Pallas kernels: 94 us -> 85.6 us
    pallas_call x1, Pallas kernels: 94 us -> 85.6 us  [local(): pl.pallas_call(kernel, out_shape=(jax.ShapeDtypeStruct((TOKENS, 2048), BF...]
where the time goes in v3:
time: 88 us; the launch traced here: 87.9 us
  Pallas kernels  85.6 us (97%)
  local copies, waits for them, and re-layouts  1.67 us (2%)
    pallas_call x1, Pallas kernels, local(): pl.pallas_call(kernel, out_shape=(jax.ShapeDtypeStruct((TOKENS, 2048), BF...  85.6 us

profile of v3, /device:TPU:1, one launch (start us, length us, event | category | flops | bytes accessed | tf_op | source)
XLA Modules:
  0.0 87.9 jit_solution(10176131013718499782)
XLA Ops:
  0.6 85.6 %filter_and_experts.1 = (bf16[256,2048]{1,0:T(8,128)(2,1)S(1)}, bf16[256,512]{1,0:T(8,128)(2,1)S(1)}) custom-call(bf16[256,1024]{1,0:T(8,128)(2,1)} %value_hbm.1, bf16[256,1024]{1,0:T(8,128)(2,1)} %gate_hbm.1, f32[31,1024]{1,0:T(8,128)} %taps_hbm.1, f32[1,1024]{1,0:T(1,128)} %bitcast.9, f32[1,1024]{1,0:T(1,128)} %bitcast.10, f32[1,1024]{1,0:T(1,128)} %bitcast.11, ...), custom_call_target="tpu_custom_call" | custom-call | tf_op jit(solution)/shard_map/filter_and_experts/pallas_call | solution.py:474
  86.3 1.0 %copy.19 = bf16[256,2048]{1,0:T(8,128)(2,1)} copy(bf16[256,2048]{1,0:T(8,128)(2,1)S(1)} %get-tuple-element.4) | data formatting | bytes 2097152
  87.2 0.7 copy.20

commit v4 on v3

--- a/solution.py
+++ b/solution.py
@@ -29,18 +29,18 @@
 )
 SCHEDULE = (
     "S9 S11 S0 S1",
-    "S12 F3 S10 F2",
-    "F1 S13 A0 F0",
-    "S14 A9 P0 P1",
-    "P2 B0 A11 S7",
-    "P3 G0 B9 A12",
-    "W0 C0 S15 B11",
-    "A10 S5 S3 B12",
-    "A13 D0 A7 B10",
-    "A14 S8 S6 B13",
-    "A15 E0 B7 C5",
-    "B14 C6 B15 D5",
-    "S4 S2 R0 D6",
+    "S12 S10 F3 S13",
+    "S14 F2 S15 S7",
+    "F1 A0 F0 S5",
+    "S3 A9 P0 P1",
+    "P2 B0 A11 P3",
+    "G0 B9 A12 W0",
+    "C0 B11 A10 S8",
+    "S6 B12 A13 D0",
+    "A7 B10 A14 S4",
+    "S2 B13 A15 E0",
+    "B7 C5 B14 C6",
+    "B15 D5 R0 D6",
     "C7 E5 C4 C3",
     "E6 D7 D4 C2",
     "C1 D3 E7 E4",
@@ -167,7 +167,7 @@
 
     for load in early[2:4]:
         load.wait()
-    lax.fori_loop(0, TOKENS // 16, normed, 0, unroll=4)
+    lax.fori_loop(0, TOKENS // 16, normed, 0)
 
     row = lax.broadcasted_iota(I32, (PLANE_ROWS, NEP), 0)
     col = lax.broadcasted_iota(I32, (PLANE_ROWS, NEP), 1)
@@ -458,6 +458,17 @@
     copy_to(first_in, first_in, rs1_send, ret_recv.at[0], to_right).wait_send()
 
 
+def hand_over(mixer_ref, out_ref, mixer_hbm, out_hbm, sem):
+    copies = [
+        pltpu.make_async_copy(mixer_ref, mixer_hbm, sem.at[0]),
+        pltpu.make_async_copy(out_ref, out_hbm, sem.at[1]),
+    ]
+    for copy in copies:
+        copy.start()
+    for copy in copies:
+        copy.wait()
+
+
 def local(
     filter_value, filter_gate, filter_taps, filter_bias, norm_gain, norm_shift, out_weight, out_bias,
     expert_input, expert_gain, route_experts, route_weights, gate_weights, up_weights, down_weights,
@@ -471,12 +482,10 @@
         gate_weights, up_weights, down_weights,
     )
     small = [argument for index, argument in enumerate(arguments[:12]) if index != 6]
-    return pl.pallas_call(
+    shapes = (jax.ShapeDtypeStruct((TOKENS, 2048), BF16), jax.ShapeDtypeStruct((TOKENS, WIDTH), BF16))
+    results = pl.pallas_call(
         kernel,
-        out_shape=(
-            jax.ShapeDtypeStruct((TOKENS, 2048), BF16),
-            jax.ShapeDtypeStruct((TOKENS, WIDTH), BF16),
-        ),
+        out_shape=shapes,
         in_specs=[hbm] * len(arguments),
         out_specs=(vmem, vmem),
         scratch_shapes=[pltpu.VMEM(argument.shape, argument.dtype) for argument in small]
@@ -510,6 +519,15 @@
         compiler_params=pltpu.CompilerParams(collective_id=0, has_side_effects=True, vmem_limit_bytes=46 * 1024 * 1024),
         name="filter_and_experts",
     )(*(pltpu.with_memory_space_constraint(argument, pltpu.HBM) for argument in arguments))
+    return pl.pallas_call(
+        hand_over,
+        out_shape=shapes,
+        in_specs=[vmem] * 2,
+        out_specs=(hbm, hbm),
+        scratch_shapes=[dma((2,))],
+        compiler_params=pltpu.CompilerParams(vmem_limit_bytes=4 * 1024 * 1024),
+        name="hand_over",
+    )(*(pltpu.with_memory_space_constraint(result, pltpu.VMEM) for result in results))
 
 
 def solution(mesh):

time: 88 us -> 86.6 us (0.984)
  local copies, waits for them, and re-layouts: 1.67 us -> 0 us
    unnamed x2 -> x0, local copies, waits for them, and re-layouts: 1.67 us -> none
    pallas_call x1 -> x2, Pallas kernels: 85.6 us -> 85.9 us  [the longest x1 84.8 us: local(): pl.pallas_call(kernel, out_shape=shapes, in_specs=[hbm] * len(arguments),...]
where the time goes in v4:
time: 86.6 us; the launch traced here: 86.5 us
  Pallas kernels  85.9 us (99%)
    pallas_call x1, Pallas kernels, local(): pl.pallas_call(kernel, out_shape=shapes, in_specs=[hbm] * len(arguments),...  84.8 us

profile of v4, /device:TPU:1, one launch (start us, length us, event | category | flops | bytes accessed | tf_op | source)
XLA Modules:
  0.0 86.5 jit_solution(6677308433484336659)
XLA Ops:
  0.6 84.8 %filter_and_experts.1 = (bf16[256,2048]{1,0:T(8,128)(2,1)S(1)}, bf16[256,512]{1,0:T(8,128)(2,1)S(1)}) custom-call(bf16[256,1024]{1,0:T(8,128)(2,1)} %value_hbm.1, bf16[256,1024]{1,0:T(8,128)(2,1)} %gate_hbm.1, f32[31,1024]{1,0:T(8,128)} %taps_hbm.1, f32[1,1024]{1,0:T(1,128)} %bitcast.9, f32[1,1024]{1,0:T(1,128)} %bitcast.10, f32[1,1024]{1,0:T(1,128)} %bitcast.11, ...), custom_call_target="tpu_custom_call" | custom-call | tf_op jit(solution)/shard_map/filter_and_experts/pallas_call | solution.py:486
  85.5 1.1 %hand_over.1 = (bf16[256,2048]{1,0:T(8,128)(2,1)}, bf16[256,512]{1,0:T(8,128)(2,1)}) custom-call(bf16[256,2048]{1,0:T(8,128)(2,1)S(1)} %get-tuple-element.4.mixer_ref, bf16[256,512]{1,0:T(8,128)(2,1)S(1)} %get-tuple-element.5.out_ref), custom_call_target="tpu_custom_call" | custom-call | tf_op jit(solution)/shard_map/hand_over/pallas_call | solution.py:522

commit v5 on v4

--- a/solution.py
+++ b/solution.py
@@ -120,8 +120,8 @@
         pl.semaphore_signal(barrier, inc=1, device_id=peer, device_id_type=MESH)
         return carry
 
-    lax.fori_loop(0, NEP // 2, greet, 0)
-    lax.fori_loop(NEP // 2 + 1, NEP, greet, 0)
+    lax.fori_loop(0, NEP // 2, greet, 0, unroll=True)
+    lax.fori_loop(NEP // 2 + 1, NEP, greet, 0, unroll=True)
     for peer in (to_right, to_left, to_after, {"ep": before // NTP, "tp": before % NTP}):
         pl.semaphore_signal(barrier, inc=1, device_id=peer, device_id_type=MESH)
 

time: 86.6 us -> 86.6 us (level)
  no operation moved by 1% of the time
where the time goes in v5:
time: 86.6 us; the launch traced here: 86.5 us
  Pallas kernels  85.8 us (99%)
    pallas_call x1, Pallas kernels, local(): pl.pallas_call(kernel, out_shape=shapes, in_specs=[hbm] * len(arguments),...  84.8 us

profile of v5, /device:TPU:1, one launch (start us, length us, event | category | flops | bytes accessed | tf_op | source)
XLA Modules:
  0.0 86.5 jit_solution(14636967041086772789)
XLA Ops:
  0.6 84.8 %filter_and_experts.1 = (bf16[256,2048]{1,0:T(8,128)(2,1)S(1)}, bf16[256,512]{1,0:T(8,128)(2,1)S(1)}) custom-call(bf16[256,1024]{1,0:T(8,128)(2,1)} %value_hbm.1, bf16[256,1024]{1,0:T(8,128)(2,1)} %gate_hbm.1, f32[31,1024]{1,0:T(8,128)} %taps_hbm.1, f32[1,1024]{1,0:T(1,128)} %bitcast.9, f32[1,1024]{1,0:T(1,128)} %bitcast.10, f32[1,1024]{1,0:T(1,128)} %bitcast.11, ...), custom_call_target="tpu_custom_call" | custom-call | tf_op jit(solution)/shard_map/filter_and_experts/pallas_call | solution.py:486
  85.4 1.1 %hand_over.1 = (bf16[256,2048]{1,0:T(8,128)(2,1)}, bf16[256,512]{1,0:T(8,128)(2,1)}) custom-call(bf16[256,2048]{1,0:T(8,128)(2,1)S(1)} %get-tuple-element.4.mixer_ref, bf16[256,512]{1,0:T(8,128)(2,1)S(1)} %get-tuple-element.5.out_ref), custom_call_target="tpu_custom_call" | custom-call | tf_op jit(solution)/shard_map/hand_over/pallas_call | solution.py:522
